TPU v7x, 512 devices: a whole 4x4x16 slice. The times are simulated.
512 devices in a mesh: sp: 128 (over z, x, core), tp: 4 (over y).
Axes of the slice: x: 4, y: 4, z: 16, core: 2. Of those that a mesh axis runs over, the one named last changes fastest.
Arguments:
- tokens: bfloat16 [65536, 2048], P('sp', 'tp'), may hold values from -6 to 6
- norm_gain: float32 [2048], replicated, may hold values from 0.1 to 1.9
- w_query: bfloat16 [2048, 1024], P('sp', 'tp'), may hold values from -1 to 1
- w_key: bfloat16 [2048, 256], P('sp', 'tp'), may hold values from -16 to 16
- w_value: bfloat16 [2048, 256], P('sp', 'tp'), may hold values from -1 to 1
- w_post_gate: bfloat16 [2048, 1024], P('sp', 'tp'), may hold values from -0.125 to 0.125
- w_pre_gate: bfloat16 [2048, 1024], P('sp', 'tp'), may hold values from -0.125 to 0.125
- w_conv_in: bfloat16 [2048, 1024], P('sp', 'tp'), may hold values from -0.125 to 0.125
- conv_taps: float32 [3, 1024], P(None, 'tp'), may hold values from -3 to 3
- sink_logit: float32 [16], P('tp'), may hold values from 2 to 6
- w_out_attn: bfloat16 [1024, 2048], P('tp', 'sp'), may hold values from -0.1875 to 0.1875
- w_out_conv: bfloat16 [1024, 2048], P('tp', 'sp'), may hold values from -0.1875 to 0.1875
Outputs:
- mixed: bfloat16 [65536, 2048], P(('sp', 'tp'))
- log_weight_sum: float32 [16, 65536], P('tp', 'sp')
All inputs are finite; a program needn't handle non-finite values.
Results may differ from a plain program's by a relative error of at most 0.012.
The roundings to bfloat16 on the way count: a program that leaves them out, or rounds other values in their place, can miss the bound.
Values may be sent and summed in bfloat16 or wider, within the bound.
No kernel may reach another device: no remote copies, remote signals or barrier semaphores. Data moves between devices by JAX's collectives and lax.ppermute only.
A program may use at most 64 MiB of HBM per device.

v0:
```python
import jax
import jax.numpy as jnp
from jax import lax
from jax.experimental import pallas as pl
from jax.experimental.pallas import tpu as pltpu
from jax.sharding import Mesh
from jax.sharding import PartitionSpec as P


HEAD_DIM = 64
WINDOW = 128
GRID_W = 64
TOKENS = 65536
SP = ("sp_0", "sp_1", "sp_2")
SP_TP = (*SP, "tp")


rope_base = 10000.0
norm_eps = 1e-06


Z, X, CORE = "sp_0", "sp_1", "sp_2"
VMEM = pl.BlockSpec(memory_space=pltpu.VMEM)
SMEM = pl.BlockSpec(memory_space=pltpu.SMEM)
PARAMS = pltpu.CompilerParams(vmem_limit_bytes=24 * 1024 * 1024)


def from_offset(x, axis, offset):
    count = lax.axis_size(axis)
    return lax.ppermute(x, axis, [((i + offset) % count, i) for i in range(count)])


def after(x, other):
    return lax.optimization_barrier((x, other))[0]


def gathered_parts(own):
    far, up, down = (from_offset(own, X, step) for step in (2, 1, 3))
    mine = (own, up, far, down)
    swapped = []
    for part in mine:
        swapped.append(from_offset(part, CORE, 1))
    return (*mine, *swapped)


def norm_kernel(gain_ref, *refs):
    tokens, normed_ref = refs[:4], refs[4]
    tp = lax.axis_index("tp")
    rows, width = tokens[0].shape
    step_rows = 64

    def norm_step(step, carry):
        at = pl.ds(pl.multiple_of(step * step_rows, step_rows), step_rows)
        blocks = [ref[at, :].astype(jnp.float32) for ref in tokens]
        square = sum(jnp.sum(b * b, axis=1, keepdims=True) for b in blocks)
        scale = lax.rsqrt(square / (4 * width) + norm_eps)
        for k, b in enumerate(blocks):
            cols = pl.ds(pl.multiple_of(lax.rem(tp + k, 4) * width, width), width)
            normed_ref[at, cols] = (b * scale * gain_ref[:, cols]).astype(jnp.bfloat16)
        return carry

    lax.fori_loop(0, rows // step_rows, norm_step, 0)


def normalized(gain, tokens):
    rows, width = tokens[0].shape
    return pl.pallas_call(
        norm_kernel,
        out_shape=jax.ShapeDtypeStruct((rows, 4 * width), jnp.bfloat16),
        in_specs=[VMEM] * 5,
        out_specs=VMEM,
        compiler_params=PARAMS,
        cost_estimate=pl.CostEstimate(
            flops=500_000_000, bytes_accessed=4_000_000, transcendentals=512
        ),
    )(gain, *tokens)


def place_rows(parts, out_ref, columns):
    x, core = lax.axis_index(X), lax.axis_index(CORE)
    for side in range(2):
        for x_rel in range(4):
            ref = parts[4 * side + x_rel]
            place = lax.rem(x + x_rel, 4) * 2 + lax.rem(core + side, 2)
            for z in range(16):
                at = pl.ds(pl.multiple_of(z * 128 + place * 16, 16), 16)
                out_ref[at, :] = ref[z, :, columns]


def rotated(x, cosine, sine):
    width = x.shape[-1]
    lane = lax.broadcasted_iota(jnp.int32, x.shape, 1)
    ahead = pltpu.roll(x, width - 16, 1)
    behind = pltpu.roll(x, 16, 1)
    return x * cosine + jnp.where(lane % 32 < 16, ahead, behind) * sine


def project_kernel(*refs):
    normed_ref, cos_ref, sin_ref = refs[:3]
    kvc_ref, query_ref, post_ref, rows_ref = refs[11:]
    place_rows(refs[3:11], rows_ref, slice(0, 1152))

    def projected(first, last):
        return jnp.dot(
            normed_ref[...], rows_ref[:, first:last], preferred_element_type=jnp.float32
        )

    key_value = projected(0, 128)
    lane = lax.broadcasted_iota(jnp.int32, key_value.shape, 1)
    cosine = cos_ref[...]
    sine = sin_ref[...]
    kvc_ref[:, :128] = jnp.where(
        lane < 64, rotated(key_value, cosine, sine), key_value
    ).astype(jnp.bfloat16)
    kvc_ref[:, 128:] = (projected(128, 384) * projected(384, 640)).astype(jnp.bfloat16)
    for half in range(2):
        part = projected(640 + 128 * half, 768 + 128 * half)
        query_ref[:, 128 * half : 128 * (half + 1)] = rotated(part, cosine, sine).astype(
            jnp.bfloat16
        )
    post_ref[...] = projected(896, 1152)


def project(normed, cosine, sine, parts):
    rows = normed.shape[0]
    return pl.pallas_call(
        project_kernel,
        out_shape=(
            jax.ShapeDtypeStruct((rows, 384), jnp.bfloat16),
            jax.ShapeDtypeStruct((rows, 256), jnp.bfloat16),
            jax.ShapeDtypeStruct((rows, 256), jnp.float32),
        ),
        in_specs=[VMEM] * 11,
        out_specs=(VMEM,) * 3,
        scratch_shapes=[pltpu.VMEM((2048, 1152), jnp.bfloat16)],
        compiler_params=PARAMS,
        cost_estimate=pl.CostEstimate(
            flops=2 * rows * 2048 * 1152, bytes_accessed=8_000_000, transcendentals=0
        ),
    )(normed, cosine, sine, *parts)


def attended_block(query, keys, values, sinks, first_key, total):
    heads = query.shape[1] // HEAD_DIM
    stacked = jnp.concatenate(
        [query[:, HEAD_DIM * h : HEAD_DIM * (h + 1)] for h in range(heads)], axis=0
    )
    scores = lax.dot_general(
        stacked, keys, (((1,), (1,)), ((), ())), preferred_element_type=jnp.float32
    ) * HEAD_DIM ** (-0.5)
    row = lax.broadcasted_iota(jnp.int32, scores.shape, 0) % WINDOW
    col = lax.broadcasted_iota(jnp.int32, scores.shape, 1)
    key_pos = first_key + col
    allowed = (col >= row) & (col <= row + 2 * WINDOW) & (key_pos >= 0) & (key_pos < total)
    scores = jnp.where(allowed, scores, -jnp.inf)
    sink = jnp.concatenate([jnp.full((WINDOW, 1), s, jnp.float32) for s in sinks], axis=0)
    row_max = jnp.maximum(jnp.max(scores, axis=1, keepdims=True), sink)
    exp_scores = jnp.exp(scores - row_max)
    denominator = jnp.sum(exp_scores, axis=1, keepdims=True) + jnp.exp(sink - row_max)
    weights = (exp_scores / denominator).astype(jnp.bfloat16)
    result = jnp.dot(weights, values, preferred_element_type=jnp.float32).astype(jnp.bfloat16)
    log_sum = row_max + jnp.log(denominator)
    by_head = [slice(WINDOW * h, WINDOW * (h + 1)) for h in range(heads)]
    return (
        jnp.concatenate([result[s] for s in by_head], axis=1),
        jnp.concatenate([log_sum[s] for s in by_head], axis=1),
    )


def first_position():
    return lax.axis_index(SP) * 512


def inner_kernel(sink_ref, query_ref, kvc_ref, *refs):
    attended_ref, log_ref, out_rows_ref = refs[8:]
    place_rows(refs[:8], out_rows_ref, slice(1152, 1664))
    sinks = [sink_ref[h] for h in range(4)]
    offset = first_position()
    for n in (1, 2):
        window = slice((n - 1) * WINDOW, (n + 2) * WINDOW)
        result, log_sum = attended_block(
            query_ref[n * WINDOW : (n + 1) * WINDOW, :],
            kvc_ref[window, :HEAD_DIM],
            kvc_ref[window, HEAD_DIM : 2 * HEAD_DIM],
            sinks,
            offset + (n - 1) * WINDOW,
            TOKENS,
        )
        attended_ref[(n - 1) * WINDOW : n * WINDOW, :] = result
        log_ref[(n - 1) * WINDOW : n * WINDOW, :] = log_sum


def inner(sinks, query, kvc, parts):
    return pl.pallas_call(
        inner_kernel,
        out_shape=(
            jax.ShapeDtypeStruct((256, 256), jnp.bfloat16),
            jax.ShapeDtypeStruct((256, 4), jnp.float32),
            jax.ShapeDtypeStruct((2048, 512), jnp.bfloat16),
        ),
        in_specs=[SMEM] + [VMEM] * 10,
        out_specs=(VMEM,) * 3,
        compiler_params=PARAMS,
        cost_estimate=pl.CostEstimate(
            flops=2 * 2 * 1024 * 384 * 64 * 20, bytes_accessed=2_000_000, transcendentals=400_000
        ),
    )(sinks, query, kvc, *parts)


def outer_kernel(
    sink_ref, query_ref, kvc_ref, low_ref, high_ref, post_ref, taps_ref, inner_ref, out_rows_ref,
    *refs,
):
    outs, log_ref, both_ref = refs[:4], refs[4], refs[5]
    sinks = [sink_ref[h] for h in range(4)]
    offset = first_position()
    rows = query_ref.shape[0]
    edges = (
        (0, jnp.concatenate([low_ref[:, :128], kvc_ref[: 2 * WINDOW, :128]], axis=0)),
        (3, jnp.concatenate([kvc_ref[rows - 2 * WINDOW :, :128], high_ref[:, :128]], axis=0)),
    )
    for k, (n, window) in enumerate(edges):
        result, log_sum = attended_block(
            query_ref[n * WINDOW : (n + 1) * WINDOW, :],
            window[:, :HEAD_DIM],
            window[:, HEAD_DIM:],
            sinks,
            offset + (n - 1) * WINDOW,
            TOKENS,
        )
        both_ref[n * WINDOW : (n + 1) * WINDOW, :256] = result
        log_ref[k * WINDOW : (k + 1) * WINDOW, :] = log_sum
    both_ref[WINDOW : 3 * WINDOW, :256] = inner_ref[...]
    conv = kvc_ref[:, 128:].astype(jnp.float32)
    row = lax.broadcasted_iota(jnp.int32, conv.shape, 0)
    before = low_ref[WINDOW - 16 :, 128:].astype(jnp.float32)[15:16]
    after = high_ref[:16, 128:].astype(jnp.float32)[0:1]
    previous = jnp.where(row == 0, before, pltpu.roll(conv, 1, 0))
    following = jnp.where(row == rows - 1, after, pltpu.roll(conv, rows - 1, 0))
    convolved = taps_ref[0:1] * previous + taps_ref[1:2] * conv + taps_ref[2:3] * following
    both_ref[:, 256:] = (post_ref[...] * convolved).astype(jnp.bfloat16)
    tp = lax.axis_index("tp")
    for step in (2, 1, 3, 0):
        at = pl.ds(pl.multiple_of(lax.rem(tp + step, 4) * WINDOW, WINDOW), WINDOW)
        outs[step][...] = lax.dot_general(
            both_ref[at, :],
            out_rows_ref[...],
            (((1,), (1,)), ((), ())),
            preferred_element_type=jnp.float32,
        ).astype(jnp.bfloat16)


def outer(sinks, query, kvc, low, high, post, taps, inner_attended, out_rows):
    return pl.pallas_call(
        outer_kernel,
        out_shape=(
            *([jax.ShapeDtypeStruct((128, 2048), jnp.bfloat16)] * 4),
            jax.ShapeDtypeStruct((256, 4), jnp.float32),
        ),
        in_specs=[SMEM] + [VMEM] * 8,
        out_specs=(VMEM,) * 5,
        scratch_shapes=[pltpu.VMEM((512, 512), jnp.bfloat16)],
        compiler_params=PARAMS,
        cost_estimate=pl.CostEstimate(
            flops=2 * 512 * 512 * 2048, bytes_accessed=8_000_000, transcendentals=400_000
        ),
    )(sinks, query, kvc, low, high, post, taps, inner_attended, out_rows)


def halo(block, width):
    count = lax.axis_size(SP)
    forward = [(i, i + 1) for i in range(count - 1)]
    backward = [(i + 1, i) for i in range(count - 1)]
    low = lax.ppermute(block[-width:], SP, forward)
    high = lax.ppermute(block[:width], SP, backward)
    return low, high


def rotation_tables(rows):
    shape = (rows, 2 * HEAD_DIM)
    lane = lax.broadcasted_iota(jnp.int32, shape, 1)
    position = lax.axis_index(SP) * rows + lax.broadcasted_iota(jnp.int32, shape, 0)
    half_dim = HEAD_DIM // 2
    inv_freq = rope_base ** (-(2 * (lane % 16)).astype(jnp.float32) / half_dim)
    index = jnp.where(lane % HEAD_DIM < half_dim, position // GRID_W, position % GRID_W)
    angle = index.astype(jnp.float32) * inv_freq
    sine = jnp.sin(angle)
    return jnp.cos(angle), jnp.where(lane % half_dim < 16, -sine, sine)


def layer(
    tokens,
    norm_gain,
    w_query,
    w_key,
    w_value,
    w_post_gate,
    w_pre_gate,
    w_conv_in,
    conv_taps,
    sink_logit,
    w_out_attn,
    w_out_conv,
):
    rows = tokens.shape[0]
    piece = jnp.concatenate(
        [
            w_key,
            w_value,
            w_pre_gate,
            w_conv_in,
            w_query,
            w_post_gate,
            w_out_attn.T,
            w_out_conv.T,
        ],
        axis=1,
    )
    own = lax.all_gather(piece, Z, axis=0)
    cosine, sine = rotation_tables(rows)
    parts = gathered_parts(own)
    late_tokens = after(tokens, own)
    arrived = [from_offset(late_tokens, "tp", step) for step in (1, 2, 3)]
    normed = normalized(norm_gain[None], [tokens, *arrived])
    kvc, query, post = project(normed, cosine, sine, parts)
    low, high = halo(kvc, WINDOW)
    inner_attended, inner_log, out_rows = inner(sink_logit, query, kvc, parts)
    *outs, outer_log = outer(
        sink_logit, query, kvc, low, high, post, conv_taps, inner_attended, out_rows
    )
    arrived = [from_offset(outs[step], "tp", -step) for step in (2, 1, 3)]
    total = outs[0].astype(jnp.float32)
    for block in arrived:
        total = total + block.astype(jnp.float32)
    log_sum = jnp.concatenate([outer_log[:WINDOW], inner_log, outer_log[WINDOW:]])
    return (total.astype(jnp.bfloat16), log_sum.T)


def solution(mesh):
    torus = Mesh(mesh.devices.reshape(16, 4, 2, mesh.shape["tp"]), SP_TP)
    return jax.shard_map(
        layer,
        mesh=torus,
        in_specs=(
            P(SP, "tp"),
            P(),
            P(SP, "tp"),
            P(SP, "tp"),
            P(SP, "tp"),
            P(SP, "tp"),
            P(SP, "tp"),
            P(SP, "tp"),
            P(None, "tp"),
            P("tp"),
            P("tp", SP),
            P("tp", SP),
        ),
        out_specs=(P(SP_TP, None), P("tp", SP)),
        check_vma=False,
    )
```

profile of v0, /device:TPU:1, one launch (start us, length us, event | category | flops | bytes accessed | tf_op | source)
XLA Modules:
  0.0 160.9 jit_solution(8760818467267421139)
XLA Ops:
  0.6 0.9 concatenate.6
  1.5 34.2 %all-gather = bf16[256,1664]{1,0:T(8,128)(2,1)S(1)} all-gather(bf16[16,1664]{1,0:T(8,128)(2,1)S(1)} %concatenate.6), channel_id=2, replica_groups=mesh['sp_0'=16,'sp_1'=4,'sp_2'=2,'tp'=4] {'sp_0'}, dimensions={0}, use_global_device_ids=true | all-gather | bytes 905216 | tf_op jit(solution)/shard_map/all_gather | solution.py:319
  35.7 3.1 %collective-permute-start.5 = (bf16[16,16,1664]{2,1,0:T(8,128)(2,1)S(1)}, bf16[16,16,1664]{2,1,0:T(8,128)(2,1)S(1)}, u32[]{:S(2)}, u32[]{:S(2)}) collective-permute-start(bf16[16,16,1664]{2,1,0:T(8,128)(2,1)S(1)} %bitcast.6), channel_id=1, source_target_pairs={{24,0},{0,8},{8,16},{16,24},{25,1},{1,9},{9,17},{17,25},{26,2},{2,... | collective-permute-start | bytes 2555912 | tf_op jit(solution)/shard_map/ppermute | solution.py:30
  38.8 4.4 %collective-permute-start.4 = (bf16[16,16,1664]{2,1,0:T(8,128)(2,1)S(1)}, bf16[16,16,1664]{2,1,0:T(8,128)(2,1)S(1)}, u32[]{:S(2)}, u32[]{:S(2)}) collective-permute-start(bf16[16,16,1664]{2,1,0:T(8,128)(2,1)S(1)} %bitcast.7), channel_id=1, source_target_pairs={{16,0},{24,8},{0,16},{8,24},{17,1},{25,9},{1,17},{9,25},{18,2},{26... | collective-permute-start | bytes 2555912 | tf_op jit(solution)/shard_map/ppermute | solution.py:30
  43.2 3.1 %collective-permute-start.3 = (bf16[16,16,1664]{2,1,0:T(8,128)(2,1)S(1)}, bf16[16,16,1664]{2,1,0:T(8,128)(2,1)S(1)}, u32[]{:S(2)}, u32[]{:S(2)}) collective-permute-start(bf16[16,16,1664]{2,1,0:T(8,128)(2,1)S(1)} %bitcast.8), channel_id=1, source_target_pairs={{8,0},{16,8},{24,16},{0,24},{9,1},{17,9},{25,17},{1,25},{10,2},{18... | collective-permute-start | bytes 2555912 | tf_op jit(solution)/shard_map/ppermute | solution.py:30
  46.3 3.2 %collective-permute-start.2 = (bf16[512,512]{1,0:T(8,128)(2,1)}, bf16[512,512]{1,0:T(8,128)(2,1)S(1)}, u32[]{:S(2)}, u32[]{:S(2)}) collective-permute-start(bf16[512,512]{1,0:T(8,128)(2,1)} %refs_0_.1), channel_id=1, source_target_pairs={{3,0},{0,1},{1,2},{2,3},{7,4},{4,5},{5,6},{6,7},{11,8},{8,9},{9,10... | collective-permute-start | bytes 1572872 | tf_op jit(solution)/shard_map/ppermute | solution.py:30
  49.5 4.5 %collective-permute-start.1 = (bf16[512,512]{1,0:T(8,128)(2,1)}, bf16[512,512]{1,0:T(8,128)(2,1)}, u32[]{:S(2)}, u32[]{:S(2)}) collective-permute-start(bf16[512,512]{1,0:T(8,128)(2,1)} %refs_0_.1), channel_id=1, source_target_pairs={{2,0},{3,1},{0,2},{1,3},{6,4},{7,5},{4,6},{5,7},{10,8},{11,9},{8,1... | collective-permute-start | bytes 1572872 | tf_op jit(solution)/shard_map/ppermute | solution.py:30
  54.0 3.9 %collective-permute-done.2.refs_3_ = bf16[512,512]{1,0:T(8,128)(2,1)S(1)} collective-permute-done((bf16[512,512]{1,0:T(8,128)(2,1)}, bf16[512,512]{1,0:T(8,128)(2,1)S(1)}, u32[]{:S(2)}, u32[]{:S(2)}) %collective-permute-start.2) | collective-permute-done | bytes 524320 | tf_op jit(solution)/shard_map/ppermute | solution.py:30
  58.0 0.8 copy-done.1
  58.8 14.7 %collective-permute-start.6 = (bf16[16,16,1664]{2,1,0:T(8,128)(2,1)S(1)}, bf16[16,16,1664]{2,1,0:T(8,128)(2,1)}, u32[]{:S(2)}, u32[]{:S(2)}) collective-permute-start(bf16[16,16,1664]{2,1,0:T(8,128)(2,1)S(1)} %bitcast.9), channel_id=1, source_target_pairs={{4,0},{0,4},{5,1},{1,5},{6,2},{2,6},{7,3},{3,7},{12,8},{8,12},{13,... | collective-permute-start | bytes 2555912 | tf_op jit(solution)/shard_map/ppermute | solution.py:30
  73.5 1.9 %collective-permute-start.9 = (bf16[16,16,1664]{2,1,0:T(8,128)(2,1)S(1)}, bf16[16,16,1664]{2,1,0:T(8,128)(2,1)}, u32[]{:S(2)}, u32[]{:S(2)}) collective-permute-start(bf16[16,16,1664]{2,1,0:T(8,128)(2,1)S(1)} %collective-permute-done.5.refs_6_.refs_3_), channel_id=1, source_target_pairs={{4,0},{0,4},{5,1},{1,5},{6,2},{2,6},{7,3},{3,7},{12,8},{8,12},{13,... | collective-permute-start | bytes 2555912 | tf_op jit(solution)/shard_map/ppermute | solution.py:30
  75.4 5.9 %collective-permute-start.8 = (bf16[16,16,1664]{2,1,0:T(8,128)(2,1)S(1)}, bf16[16,16,1664]{2,1,0:T(8,128)(2,1)}, u32[]{:S(2)}, u32[]{:S(2)}) collective-permute-start(bf16[16,16,1664]{2,1,0:T(8,128)(2,1)S(1)} %collective-permute-done.4.refs_5_.refs_2_), channel_id=1, source_target_pairs={{4,0},{0,4},{5,1},{1,5},{6,2},{2,6},{7,3},{3,7},{12,8},{8,12},{13,... | collective-permute-start | bytes 2555912 | tf_op jit(solution)/shard_map/ppermute | solution.py:30
  81.3 1.9 %collective-permute-start.7 = (bf16[16,16,1664]{2,1,0:T(8,128)(2,1)S(1)}, bf16[16,16,1664]{2,1,0:T(8,128)(2,1)}, u32[]{:S(2)}, u32[]{:S(2)}) collective-permute-start(bf16[16,16,1664]{2,1,0:T(8,128)(2,1)S(1)} %collective-permute-done.3.refs_4_.refs_1_), channel_id=1, source_target_pairs={{4,0},{0,4},{5,1},{1,5},{6,2},{2,6},{7,3},{3,7},{12,8},{8,12},{13,... | collective-permute-start | bytes 2555912 | tf_op jit(solution)/shard_map/ppermute | solution.py:30
  83.3 4.6 %collective-permute-start = (bf16[512,512]{1,0:T(8,128)(2,1)}, bf16[512,512]{1,0:T(8,128)(2,1)S(1)}, u32[]{:S(2)}, u32[]{:S(2)}) collective-permute-start(bf16[512,512]{1,0:T(8,128)(2,1)} %refs_0_.1), channel_id=1, source_target_pairs={{1,0},{2,1},{3,2},{0,3},{5,4},{6,5},{7,6},{4,7},{9,8},{10,9},{11,1... | collective-permute-start | bytes 1572872 | tf_op jit(solution)/shard_map/ppermute | solution.py:30
  88.0 1.1 negate_select_fusion
  89.1 10.0 %collective-permute-done.refs_1_ = bf16[512,512]{1,0:T(8,128)(2,1)S(1)} collective-permute-done((bf16[512,512]{1,0:T(8,128)(2,1)}, bf16[512,512]{1,0:T(8,128)(2,1)S(1)}, u32[]{:S(2)}, u32[]{:S(2)}) %collective-permute-start) | collective-permute-done | bytes 524320 | tf_op jit(solution)/shard_map/ppermute | solution.py:30
  99.0 1.0 copy-done
  100.1 1.0 copy-done.2
  101.1 0.7 copy-done.3
  101.8 2.5 %shard_map.131.refs_0_ = bf16[512,2048]{1,0:T(8,128)(2,1)S(1)} custom-call(f32[1,2048]{1,0:T(1,128)S(1)} %bitcast.12, bf16[512,512]{1,0:T(8,128)(2,1)S(1)} %copy-done, bf16[512,512]{1,0:T(8,128)(2,1)S(1)} %collective-permute-done.refs_1_, bf16[512,512]{1,0:T(8,128)(2,1)} %collective-permute-done.1.refs_2_, bf16[512,512]{1,0:T(8,128)(2,1)S(1)} %copy-done.2), custom_call_target="tpu_custom_call" | custom-call | flops 500000000 | bytes 4000000 | tf_op jit(solution)/shard_map/pallas_call | solution.py:67
  104.4 5.8 %shard_map.132 = (bf16[512,384]{1,0:T(8,128)(2,1)S(1)}, bf16[512,256]{1,0:T(8,128)(2,1)S(1)}, f32[512,256]{1,0:T(8,128)S(1)}) custom-call(bf16[512,2048]{1,0:T(8,128)(2,1)S(1)} %shard_map.131.refs_0_, f32[512,128]{1,0:T(8,128)S(1)} %get-tuple-element.33.refs_1_, f32[512,128]{1,0:T(8,128)S(1)} %get-tuple-element.32.refs_2_, ...), custom_call_target="tpu_custom_call" | custom-call | flops 2415919104 | bytes 8000000 | tf_op jit(solution)/shard_map/pallas_call | solution.py:126
  110.1 3.3 %collective-permute-start.11 = (bf16[128,384]{1,0:T(8,128)(2,1)S(1)}, bf16[128,384]{1,0:T(8,128)(2,1)S(1)}, u32[]{:S(2)}, u32[]{:S(2)}) collective-permute-start(bf16[128,384]{1,0:T(8,128)(2,1)S(1)} %get-tuple-element.28), channel_id=1, source_target_pairs={{4,0},{8,4},{12,8},{16,12},{20,16},{24,20},{28,24},{32,28},{36,32}... | collective-permute-start | bytes 294920 | tf_op jit(solution)/shard_map/ppermute | solution.py:275
  113.4 3.5 %collective-permute-start.10 = (bf16[128,384]{1,0:T(8,128)(2,1)S(1)}, bf16[128,384]{1,0:T(8,128)(2,1)S(1)}, u32[]{:S(2)}, u32[]{:S(2)}) collective-permute-start(bf16[128,384]{1,0:T(8,128)(2,1)S(1)} %get-tuple-element.29), channel_id=1, source_target_pairs={{0,4},{4,8},{8,12},{12,16},{16,20},{20,24},{24,28},{28,32},{32,36}... | collective-permute-start | bytes 294920 | tf_op jit(solution)/shard_map/ppermute | solution.py:274
  117.0 5.3 %shard_map.133 = (bf16[256,256]{1,0:T(8,128)(2,1)S(1)}, f32[256,4]{1,0:T(8,128)S(1)}, bf16[2048,512]{1,0:T(8,128)(2,1)S(1)}) custom-call(f32[4]{0:T(128)S(1)} %copy-done.4, bf16[512,256]{1,0:T(8,128)(2,1)S(1)} %get-tuple-element.15.query_ref, bf16[512,384]{1,0:T(8,128)(2,1)S(1)} %get-tuple-element.16.kvc_ref, bf16[16,16,1664]{2,1,0:T(8,128)(2,1)S(1)} %bitcast.11, ...), custom_call_target="tpu_custom_call" | custom-call | flops 2013265920 | bytes 2000000 | tf_op jit(solution)/shard_map/pallas_call | solution.py:194
  122.3 7.7 %shard_map.134 = (bf16[128,2048]{1,0:T(8,128)(2,1)S(1)}, bf16[128,2048]{1,0:T(8,128)(2,1)S(1)}, bf16[128,2048]{1,0:T(8,128)(2,1)S(1)}, bf16[128,2048]{1,0:T(8,128)(2,1)S(1)}, f32[256,4]{1,0:T(8,128)S(1)}) custom-call(f32[4]{0:T(128)S(1)} %copy-done.4, bf16[512,256]{1,0:T(8,128)(2,1)S(1)} %get-tuple-element.15.query_ref, ...), custom_call_target="tpu_custom_call" | custom-call | flops 1073741824 | bytes 8000000 | tf_op jit(solution)/shard_map/pallas_call | solution.py:254
  130.1 4.2 %collective-permute-start.12 = (bf16[128,2048]{1,0:T(8,128)(2,1)S(1)}, bf16[128,2048]{1,0:T(8,128)(2,1)S(1)}, u32[]{:S(2)}, u32[]{:S(2)}) collective-permute-start(bf16[128,2048]{1,0:T(8,128)(2,1)S(1)} %get-tuple-element.21), channel_id=1, source_target_pairs={{2,0},{3,1},{0,2},{1,3},{6,4},{7,5},{4,6},{5,7},{10,8},{11,9},{8,1... | collective-permute-start | bytes 1572872 | tf_op jit(solution)/shard_map/ppermute | solution.py:30
  134.2 3.5 %collective-permute-start.13 = (bf16[128,2048]{1,0:T(8,128)(2,1)S(1)}, bf16[128,2048]{1,0:T(8,128)(2,1)S(1)}, u32[]{:S(2)}, u32[]{:S(2)}) collective-permute-start(bf16[128,2048]{1,0:T(8,128)(2,1)S(1)} %get-tuple-element.22), channel_id=1, source_target_pairs={{3,0},{0,1},{1,2},{2,3},{7,4},{4,5},{5,6},{6,7},{11,8},{8,9},{9,10... | collective-permute-start | bytes 1572872 | tf_op jit(solution)/shard_map/ppermute | solution.py:30
  137.8 3.0 %collective-permute-start.14 = (bf16[128,2048]{1,0:T(8,128)(2,1)S(1)}, bf16[128,2048]{1,0:T(8,128)(2,1)}, u32[]{:S(2)}, u32[]{:S(2)}) collective-permute-start(bf16[128,2048]{1,0:T(8,128)(2,1)S(1)} %get-tuple-element.23), channel_id=1, source_target_pairs={{1,0},{2,1},{3,2},{0,3},{5,4},{6,5},{7,6},{4,7},{9,8},{10,9},{11,1... | collective-permute-start | bytes 1572872 | tf_op jit(solution)/shard_map/ppermute | solution.py:30
  141.6 5.5 %collective-permute-done.12 = bf16[128,2048]{1,0:T(8,128)(2,1)S(1)} collective-permute-done((bf16[128,2048]{1,0:T(8,128)(2,1)S(1)}, bf16[128,2048]{1,0:T(8,128)(2,1)S(1)}, u32[]{:S(2)}, u32[]{:S(2)}) %collective-permute-start.12) | collective-permute-done | bytes 524320 | tf_op jit(solution)/shard_map/ppermute | solution.py:30
  147.2 10.8 %collective-permute-done.13 = bf16[128,2048]{1,0:T(8,128)(2,1)S(1)} collective-permute-done((bf16[128,2048]{1,0:T(8,128)(2,1)S(1)}, bf16[128,2048]{1,0:T(8,128)(2,1)S(1)}, u32[]{:S(2)}, u32[]{:S(2)}) %collective-permute-start.13) | collective-permute-done | bytes 524320 | tf_op jit(solution)/shard_map/ppermute | solution.py:30
  158.0 0.8 collective-permute-done.14
  158.8 2.2 %add_convert_fusion = bf16[128,2048]{1,0:T(8,128)(2,1)} fusion(bf16[128,2048]{1,0:T(8,128)(2,1)} %collective-permute-done.14, bf16[128,2048]{1,0:T(8,128)(2,1)S(1)} %collective-permute-done.13, bf16[128,2048]{1,0:T(8,128)(2,1)S(1)} %collective-permute-done.12, bf16[128,2048]{1,0:T(8,128)(2,1)S(1)} %get-tuple-element.20), kind=kLoop, calls=%fused_computation | loop fusion | flops 2097152 | bytes 2621440 | tf_op jit(solution)/shard_map/convert_element_type | solution.py:336
  (32 shorter events, 1.0 us)
Async XLA Ops:
  35.7 37.8 %collective-permute-start.5 = (bf16[16,16,1664]{2,1,0:T(8,128)(2,1)S(1)}, bf16[16,16,1664]{2,1,0:T(8,128)(2,1)S(1)}, u32[]{:S(2)}, u32[]{:S(2)}) collective-permute-start(bf16[16,16,1664]{2,1,0:T(8,128)(2,1)S(1)} %bitcast.6), channel_id=1, source_target_pairs={{24,0},{0,8},{8,16},{16,24},{25,1},{1,9},{9,17},{17,25},{26,2},{2,... | collective-permute-start | bytes 2555912 | tf_op jit(solution)/shard_map/ppermute | solution.py:30
  38.8 36.6 %collective-permute-start.4 = (bf16[16,16,1664]{2,1,0:T(8,128)(2,1)S(1)}, bf16[16,16,1664]{2,1,0:T(8,128)(2,1)S(1)}, u32[]{:S(2)}, u32[]{:S(2)}) collective-permute-start(bf16[16,16,1664]{2,1,0:T(8,128)(2,1)S(1)} %bitcast.7), channel_id=1, source_target_pairs={{16,0},{24,8},{0,16},{8,24},{17,1},{25,9},{1,17},{9,25},{18,2},{26... | collective-permute-start | bytes 2555912 | tf_op jit(solution)/shard_map/ppermute | solution.py:30
  43.2 38.1 %collective-permute-start.3 = (bf16[16,16,1664]{2,1,0:T(8,128)(2,1)S(1)}, bf16[16,16,1664]{2,1,0:T(8,128)(2,1)S(1)}, u32[]{:S(2)}, u32[]{:S(2)}) collective-permute-start(bf16[16,16,1664]{2,1,0:T(8,128)(2,1)S(1)} %bitcast.8), channel_id=1, source_target_pairs={{8,0},{16,8},{24,16},{0,24},{9,1},{17,9},{25,17},{1,25},{10,2},{18... | collective-permute-start | bytes 2555912 | tf_op jit(solution)/shard_map/ppermute | solution.py:30
  46.3 11.7 %collective-permute-start.2 = (bf16[512,512]{1,0:T(8,128)(2,1)}, bf16[512,512]{1,0:T(8,128)(2,1)S(1)}, u32[]{:S(2)}, u32[]{:S(2)}) collective-permute-start(bf16[512,512]{1,0:T(8,128)(2,1)} %refs_0_.1), channel_id=1, source_target_pairs={{3,0},{0,1},{1,2},{2,3},{7,4},{4,5},{5,6},{6,7},{11,8},{8,9},{9,10... | collective-permute-start | bytes 1572872 | tf_op jit(solution)/shard_map/ppermute | solution.py:30
  49.5 33.8 %collective-permute-start.1 = (bf16[512,512]{1,0:T(8,128)(2,1)}, bf16[512,512]{1,0:T(8,128)(2,1)}, u32[]{:S(2)}, u32[]{:S(2)}) collective-permute-start(bf16[512,512]{1,0:T(8,128)(2,1)} %refs_0_.1), channel_id=1, source_target_pairs={{2,0},{3,1},{0,2},{1,3},{6,4},{7,5},{4,6},{5,7},{10,8},{11,9},{8,1... | collective-permute-start | bytes 1572872 | tf_op jit(solution)/shard_map/ppermute | solution.py:30
  58.0 0.8 copy-start.1
  58.8 45.5 %collective-permute-start.6 = (bf16[16,16,1664]{2,1,0:T(8,128)(2,1)S(1)}, bf16[16,16,1664]{2,1,0:T(8,128)(2,1)}, u32[]{:S(2)}, u32[]{:S(2)}) collective-permute-start(bf16[16,16,1664]{2,1,0:T(8,128)(2,1)S(1)} %bitcast.9), channel_id=1, source_target_pairs={{4,0},{0,4},{5,1},{1,5},{6,2},{2,6},{7,3},{3,7},{12,8},{8,12},{13,... | collective-permute-start | bytes 2555912 | tf_op jit(solution)/shard_map/ppermute | solution.py:30
  73.5 30.8 %collective-permute-start.9 = (bf16[16,16,1664]{2,1,0:T(8,128)(2,1)S(1)}, bf16[16,16,1664]{2,1,0:T(8,128)(2,1)}, u32[]{:S(2)}, u32[]{:S(2)}) collective-permute-start(bf16[16,16,1664]{2,1,0:T(8,128)(2,1)S(1)} %collective-permute-done.5.refs_6_.refs_3_), channel_id=1, source_target_pairs={{4,0},{0,4},{5,1},{1,5},{6,2},{2,6},{7,3},{3,7},{12,8},{8,12},{13,... | collective-permute-start | bytes 2555912 | tf_op jit(solution)/shard_map/ppermute | solution.py:30
  75.4 28.9 %collective-permute-start.8 = (bf16[16,16,1664]{2,1,0:T(8,128)(2,1)S(1)}, bf16[16,16,1664]{2,1,0:T(8,128)(2,1)}, u32[]{:S(2)}, u32[]{:S(2)}) collective-permute-start(bf16[16,16,1664]{2,1,0:T(8,128)(2,1)S(1)} %collective-permute-done.4.refs_5_.refs_2_), channel_id=1, source_target_pairs={{4,0},{0,4},{5,1},{1,5},{6,2},{2,6},{7,3},{3,7},{12,8},{8,12},{13,... | collective-permute-start | bytes 2555912 | tf_op jit(solution)/shard_map/ppermute | solution.py:30
  81.3 23.0 %collective-permute-start.7 = (bf16[16,16,1664]{2,1,0:T(8,128)(2,1)S(1)}, bf16[16,16,1664]{2,1,0:T(8,128)(2,1)}, u32[]{:S(2)}, u32[]{:S(2)}) collective-permute-start(bf16[16,16,1664]{2,1,0:T(8,128)(2,1)S(1)} %collective-permute-done.3.refs_4_.refs_1_), channel_id=1, source_target_pairs={{4,0},{0,4},{5,1},{1,5},{6,2},{2,6},{7,3},{3,7},{12,8},{8,12},{13,... | collective-permute-start | bytes 2555912 | tf_op jit(solution)/shard_map/ppermute | solution.py:30
  83.3 15.7 %collective-permute-start = (bf16[512,512]{1,0:T(8,128)(2,1)}, bf16[512,512]{1,0:T(8,128)(2,1)S(1)}, u32[]{:S(2)}, u32[]{:S(2)}) collective-permute-start(bf16[512,512]{1,0:T(8,128)(2,1)} %refs_0_.1), channel_id=1, source_target_pairs={{1,0},{2,1},{3,2},{0,3},{5,4},{6,5},{7,6},{4,7},{9,8},{10,9},{11,1... | collective-permute-start | bytes 1572872 | tf_op jit(solution)/shard_map/ppermute | solution.py:30
  99.0 1.0 copy-start
  100.1 1.0 copy-start.2
  101.1 0.7 copy-start.3
  104.3 12.6 %copy-start.4 = (f32[4]{0:T(128)S(1)}, f32[4]{0:T(128)}, u32[]{:S(2)}) copy-start(f32[4]{0:T(128)} %sink_ref.3) | copy-start | bytes 52
  110.1 12.2 %collective-permute-start.11 = (bf16[128,384]{1,0:T(8,128)(2,1)S(1)}, bf16[128,384]{1,0:T(8,128)(2,1)S(1)}, u32[]{:S(2)}, u32[]{:S(2)}) collective-permute-start(bf16[128,384]{1,0:T(8,128)(2,1)S(1)} %get-tuple-element.28), channel_id=1, source_target_pairs={{4,0},{8,4},{12,8},{16,12},{20,16},{24,20},{28,24},{32,28},{36,32}... | collective-permute-start | bytes 294920 | tf_op jit(solution)/shard_map/ppermute | solution.py:275
  113.4 8.9 %collective-permute-start.10 = (bf16[128,384]{1,0:T(8,128)(2,1)S(1)}, bf16[128,384]{1,0:T(8,128)(2,1)S(1)}, u32[]{:S(2)}, u32[]{:S(2)}) collective-permute-start(bf16[128,384]{1,0:T(8,128)(2,1)S(1)} %get-tuple-element.29), channel_id=1, source_target_pairs={{0,4},{4,8},{8,12},{12,16},{16,20},{20,24},{24,28},{28,32},{32,36}... | collective-permute-start | bytes 294920 | tf_op jit(solution)/shard_map/ppermute | solution.py:274
  116.9 5.4 %copy-start.5 = (f32[3,256]{1,0:T(4,128)S(1)}, f32[3,256]{1,0:T(4,128)}, u32[]{:S(2)}) copy-start(f32[3,256]{1,0:T(4,128)} %taps_ref.1) | copy-start | bytes 9220
  130.1 17.1 %collective-permute-start.12 = (bf16[128,2048]{1,0:T(8,128)(2,1)S(1)}, bf16[128,2048]{1,0:T(8,128)(2,1)S(1)}, u32[]{:S(2)}, u32[]{:S(2)}) collective-permute-start(bf16[128,2048]{1,0:T(8,128)(2,1)S(1)} %get-tuple-element.21), channel_id=1, source_target_pairs={{2,0},{3,1},{0,2},{1,3},{6,4},{7,5},{4,6},{5,7},{10,8},{11,9},{8,1... | collective-permute-start | bytes 1572872 | tf_op jit(solution)/shard_map/ppermute | solution.py:30
  134.2 23.7 %collective-permute-start.13 = (bf16[128,2048]{1,0:T(8,128)(2,1)S(1)}, bf16[128,2048]{1,0:T(8,128)(2,1)S(1)}, u32[]{:S(2)}, u32[]{:S(2)}) collective-permute-start(bf16[128,2048]{1,0:T(8,128)(2,1)S(1)} %get-tuple-element.22), channel_id=1, source_target_pairs={{3,0},{0,1},{1,2},{2,3},{7,4},{4,5},{5,6},{6,7},{11,8},{8,9},{9,10... | collective-permute-start | bytes 1572872 | tf_op jit(solution)/shard_map/ppermute | solution.py:30
  137.8 21.0 %collective-permute-start.14 = (bf16[128,2048]{1,0:T(8,128)(2,1)S(1)}, bf16[128,2048]{1,0:T(8,128)(2,1)}, u32[]{:S(2)}, u32[]{:S(2)}) collective-permute-start(bf16[128,2048]{1,0:T(8,128)(2,1)S(1)} %get-tuple-element.23), channel_id=1, source_target_pairs={{1,0},{2,1},{3,2},{0,3},{5,4},{6,5},{7,6},{4,7},{9,8},{10,9},{11,1... | collective-permute-start | bytes 1572872 | tf_op jit(solution)/shard_map/ppermute | solution.py:30
where the time goes:
time: 162 us; the launch traced here: 161 us
  starting transfers between devices  64.8 us (40%)
  blocking collectives  34.2 us (21%)
  waiting for transfers between devices  31.1 us (19%)
  Pallas kernels  21.3 us (13%)
  local copies, waits for them, and re-layouts  4.73 us (3%)
  other arithmetic  3.93 us (2%)
    ppermute x13, starting transfers between devices, from_offset(): lax.ppermute(x, axis, [((i + offset) % count, i) for i in range(count)])  58 us
    all_gather x1, blocking collectives, layer(): own = lax.all_gather(piece, Z, axis=0)  34.2 us
    ppermute x13, waiting for transfers between devices, from_offset(): lax.ppermute(x, axis, [((i + offset) % count, i) for i in range(count)])  31.1 us
    pallas_call x1, Pallas kernels, outer(): pl.pallas_call(outer_kernel, out_shape=(*[jax.ShapeDtypeStruct((128, 2048...  7.73 us
    pallas_call x1, Pallas kernels, project(): pl.pallas_call(project_kernel, out_shape=(jax.ShapeDtypeStruct((rows, 384...  5.76 us
    pallas_call x1, Pallas kernels, inner(): pl.pallas_call(inner_kernel, out_shape=(jax.ShapeDtypeStruct((256, 256),...  5.33 us
    unnamed x12, local copies, waits for them, and re-layouts  3.58 us
    ppermute x1, starting transfers between devices, halo(): low = lax.ppermute(block[-width:], SP, forward)  3.51 us
  transfers between devices with their start and end apart: 15, of which 5 were waited for; matrix products, arithmetic and copies ran while one was open for 1% of the time, Pallas kernels for 5%

commit v1 on v0

--- a/solution.py
+++ b/solution.py
@@ -22,7 +22,10 @@
 Z, X, CORE = "sp_0", "sp_1", "sp_2"
 VMEM = pl.BlockSpec(memory_space=pltpu.VMEM)
 SMEM = pl.BlockSpec(memory_space=pltpu.SMEM)
-PARAMS = pltpu.CompilerParams(vmem_limit_bytes=24 * 1024 * 1024)
+
+
+def params(mib):
+    return pltpu.CompilerParams(vmem_limit_bytes=mib * 1024 * 1024)
 
 
 def from_offset(x, axis, offset):
@@ -69,7 +72,7 @@
         out_shape=jax.ShapeDtypeStruct((rows, 4 * width), jnp.bfloat16),
         in_specs=[VMEM] * 5,
         out_specs=VMEM,
-        compiler_params=PARAMS,
+        compiler_params=params(8),
         cost_estimate=pl.CostEstimate(
             flops=500_000_000, bytes_accessed=4_000_000, transcendentals=512
         ),
@@ -133,37 +136,46 @@
         in_specs=[VMEM] * 11,
         out_specs=(VMEM,) * 3,
         scratch_shapes=[pltpu.VMEM((2048, 1152), jnp.bfloat16)],
-        compiler_params=PARAMS,
+        compiler_params=params(24),
         cost_estimate=pl.CostEstimate(
             flops=2 * rows * 2048 * 1152, bytes_accessed=8_000_000, transcendentals=0
         ),
     )(normed, cosine, sine, *parts)
 
 
-def attended_block(query, keys, values, sinks, first_key, total):
+def window_bias():
+    row = lax.broadcasted_iota(jnp.int32, (WINDOW, 3 * WINDOW), 0)
+    col = lax.broadcasted_iota(jnp.int32, (WINDOW, 3 * WINDOW), 1)
+    return jnp.where((col >= row) & (col <= row + 2 * WINDOW), 0.0, -jnp.inf)
+
+
+def inside_sequence(bias, first_key):
+    key_pos = first_key + lax.broadcasted_iota(jnp.int32, bias.shape, 1)
+    return jnp.where((key_pos >= 0) & (key_pos < TOKENS), bias, -jnp.inf)
+
+
+def attended_block(query, keys, values, sinks, bias):
     heads = query.shape[1] // HEAD_DIM
+    query = query * jnp.bfloat16(HEAD_DIM**-0.5)
     stacked = jnp.concatenate(
         [query[:, HEAD_DIM * h : HEAD_DIM * (h + 1)] for h in range(heads)], axis=0
     )
     scores = lax.dot_general(
         stacked, keys, (((1,), (1,)), ((), ())), preferred_element_type=jnp.float32
-    ) * HEAD_DIM ** (-0.5)
-    row = lax.broadcasted_iota(jnp.int32, scores.shape, 0) % WINDOW
-    col = lax.broadcasted_iota(jnp.int32, scores.shape, 1)
-    key_pos = first_key + col
-    allowed = (col >= row) & (col <= row + 2 * WINDOW) & (key_pos >= 0) & (key_pos < total)
-    scores = jnp.where(allowed, scores, -jnp.inf)
-    sink = jnp.concatenate([jnp.full((WINDOW, 1), s, jnp.float32) for s in sinks], axis=0)
-    row_max = jnp.maximum(jnp.max(scores, axis=1, keepdims=True), sink)
-    exp_scores = jnp.exp(scores - row_max)
-    denominator = jnp.sum(exp_scores, axis=1, keepdims=True) + jnp.exp(sink - row_max)
-    weights = (exp_scores / denominator).astype(jnp.bfloat16)
+    )
+    results, logs = [], []
+    for h in range(heads):
+        own = scores[WINDOW * h : WINDOW * (h + 1)] + bias
+        row_max = jnp.maximum(jnp.max(own, axis=1, keepdims=True), sinks[h])
+        exp_scores = jnp.exp(own - row_max)
+        denominator = jnp.sum(exp_scores, axis=1, keepdims=True) + jnp.exp(sinks[h] - row_max)
+        results.append((exp_scores * (1.0 / denominator)).astype(jnp.bfloat16))
+        logs.append(row_max + jnp.log(denominator))
+    weights = jnp.concatenate(results, axis=0)
     result = jnp.dot(weights, values, preferred_element_type=jnp.float32).astype(jnp.bfloat16)
-    log_sum = row_max + jnp.log(denominator)
-    by_head = [slice(WINDOW * h, WINDOW * (h + 1)) for h in range(heads)]
     return (
-        jnp.concatenate([result[s] for s in by_head], axis=1),
-        jnp.concatenate([log_sum[s] for s in by_head], axis=1),
+        jnp.concatenate([result[WINDOW * h : WINDOW * (h + 1)] for h in range(heads)], axis=1),
+        jnp.concatenate(logs, axis=1),
     )
 
 
@@ -175,7 +187,7 @@
     attended_ref, log_ref, out_rows_ref = refs[8:]
     place_rows(refs[:8], out_rows_ref, slice(1152, 1664))
     sinks = [sink_ref[h] for h in range(4)]
-    offset = first_position()
+    bias = window_bias()
     for n in (1, 2):
         window = slice((n - 1) * WINDOW, (n + 2) * WINDOW)
         result, log_sum = attended_block(
@@ -183,8 +195,7 @@
             kvc_ref[window, :HEAD_DIM],
             kvc_ref[window, HEAD_DIM : 2 * HEAD_DIM],
             sinks,
-            offset + (n - 1) * WINDOW,
-            TOKENS,
+            bias,
         )
         attended_ref[(n - 1) * WINDOW : n * WINDOW, :] = result
         log_ref[(n - 1) * WINDOW : n * WINDOW, :] = log_sum
@@ -200,7 +211,7 @@
         ),
         in_specs=[SMEM] + [VMEM] * 10,
         out_specs=(VMEM,) * 3,
-        compiler_params=PARAMS,
+        compiler_params=params(12),
         cost_estimate=pl.CostEstimate(
             flops=2 * 2 * 1024 * 384 * 64 * 20, bytes_accessed=2_000_000, transcendentals=400_000
         ),
@@ -211,9 +222,10 @@
     sink_ref, query_ref, kvc_ref, low_ref, high_ref, post_ref, taps_ref, inner_ref, out_rows_ref,
     *refs,
 ):
-    outs, log_ref, both_ref = refs[:4], refs[4], refs[5]
+    far_ref, both_ref, log_ref = refs
     sinks = [sink_ref[h] for h in range(4)]
     offset = first_position()
+    bias = window_bias()
     rows = query_ref.shape[0]
     edges = (
         (0, jnp.concatenate([low_ref[:, :128], kvc_ref[: 2 * WINDOW, :128]], axis=0)),
@@ -225,8 +237,7 @@
             window[:, :HEAD_DIM],
             window[:, HEAD_DIM:],
             sinks,
-            offset + (n - 1) * WINDOW,
-            TOKENS,
+            inside_sequence(bias, offset + (n - 1) * WINDOW),
         )
         both_ref[n * WINDOW : (n + 1) * WINDOW, :256] = result
         log_ref[k * WINDOW : (k + 1) * WINDOW, :] = log_sum
@@ -239,28 +250,52 @@
     following = jnp.where(row == rows - 1, after, pltpu.roll(conv, rows - 1, 0))
     convolved = taps_ref[0:1] * previous + taps_ref[1:2] * conv + taps_ref[2:3] * following
     both_ref[:, 256:] = (post_ref[...] * convolved).astype(jnp.bfloat16)
-    tp = lax.axis_index("tp")
-    for step in (2, 1, 3, 0):
-        at = pl.ds(pl.multiple_of(lax.rem(tp + step, 4) * WINDOW, WINDOW), WINDOW)
-        outs[step][...] = lax.dot_general(
-            both_ref[at, :],
-            out_rows_ref[...],
-            (((1,), (1,)), ((), ())),
-            preferred_element_type=jnp.float32,
-        ).astype(jnp.bfloat16)
+    send_chunk(both_ref, out_rows_ref, far_ref, 2)
+
+
+def send_chunk(both_ref, out_rows_ref, out_ref, step):
+    block = lax.rem(lax.axis_index("tp") + step, 4)
+    out_ref[...] = lax.dot_general(
+        both_ref[pl.ds(pl.multiple_of(block * WINDOW, WINDOW), WINDOW), :],
+        out_rows_ref[...],
+        (((1,), (1,)), ((), ())),
+        preferred_element_type=jnp.float32,
+    ).astype(jnp.bfloat16)
+
+
+def near_kernel(both_ref, out_rows_ref, up_ref, down_ref):
+    send_chunk(both_ref, out_rows_ref, up_ref, 1)
+    send_chunk(both_ref, out_rows_ref, down_ref, 3)
+
+
+def own_kernel(both_ref, out_rows_ref, own_ref):
+    send_chunk(both_ref, out_rows_ref, own_ref, 0)
+
+
+def chunks(kernel, count, both, out_rows):
+    return pl.pallas_call(
+        kernel,
+        out_shape=(jax.ShapeDtypeStruct((128, 2048), jnp.bfloat16),) * count,
+        in_specs=[VMEM] * 2,
+        out_specs=(VMEM,) * count,
+        compiler_params=params(12),
+        cost_estimate=pl.CostEstimate(
+            flops=count * 2 * 128 * 512 * 2048, bytes_accessed=3_000_000, transcendentals=0
+        ),
+    )(both, out_rows)
 
 
 def outer(sinks, query, kvc, low, high, post, taps, inner_attended, out_rows):
     return pl.pallas_call(
         outer_kernel,
         out_shape=(
-            *([jax.ShapeDtypeStruct((128, 2048), jnp.bfloat16)] * 4),
+            jax.ShapeDtypeStruct((128, 2048), jnp.bfloat16),
+            jax.ShapeDtypeStruct((512, 512), jnp.bfloat16),
             jax.ShapeDtypeStruct((256, 4), jnp.float32),
         ),
         in_specs=[SMEM] + [VMEM] * 8,
-        out_specs=(VMEM,) * 5,
-        scratch_shapes=[pltpu.VMEM((512, 512), jnp.bfloat16)],
-        compiler_params=PARAMS,
+        out_specs=(VMEM,) * 3,
+        compiler_params=params(8),
         cost_estimate=pl.CostEstimate(
             flops=2 * 512 * 512 * 2048, bytes_accessed=8_000_000, transcendentals=400_000
         ),
@@ -321,15 +356,18 @@
     parts = gathered_parts(own)
     late_tokens = after(tokens, own)
     arrived = [from_offset(late_tokens, "tp", step) for step in (1, 2, 3)]
-    normed = normalized(norm_gain[None], [tokens, *arrived])
+    normed = normalized(after(norm_gain[None], (cosine, sine)), [tokens, *arrived])
     kvc, query, post = project(normed, cosine, sine, parts)
     low, high = halo(kvc, WINDOW)
     inner_attended, inner_log, out_rows = inner(sink_logit, query, kvc, parts)
-    *outs, outer_log = outer(
+    far, both, outer_log = outer(
         sink_logit, query, kvc, low, high, post, conv_taps, inner_attended, out_rows
     )
-    arrived = [from_offset(outs[step], "tp", -step) for step in (2, 1, 3)]
-    total = outs[0].astype(jnp.float32)
+    arrived = [from_offset(far, "tp", -2)]
+    up, down = chunks(near_kernel, 2, both, out_rows)
+    arrived += [from_offset(up, "tp", -1), from_offset(down, "tp", -3)]
+    (mine,) = chunks(own_kernel, 1, both, out_rows)
+    total = mine.astype(jnp.float32)
     for block in arrived:
         total = total + block.astype(jnp.float32)
     log_sum = jnp.concatenate([outer_log[:WINDOW], inner_log, outer_log[WINDOW:]])

time: 162 us -> 162 us (level)
  Pallas kernels: 21.3 us -> 19.1 us
    pallas_call x1 -> x3, Pallas kernels: 7.73 us -> 6.82 us  [the longest x1 3.7 us: outer(): pl.pallas_call(outer_kernel, out_shape=(jax.ShapeDtypeStruct((128, 2048),...]
    unnamed x12 -> x16, local copies, waits for them, and re-layouts: 3.58 us -> 4.06 us
  transfers between devices with their start and end apart: 15 -> 15, of which waited for: 5 -> 4; matrix products, arithmetic and copies ran while one was open for 1% -> 1% of each run, Pallas kernels for 5% -> 4%
where the time goes in v1:
time: 162 us; the launch traced here: 161 us
  starting transfers between devices  65.2 us (40%)
  blocking collectives  34.2 us (21%)
  waiting for transfers between devices  31.7 us (20%)
  Pallas kernels  19.1 us (12%)
  local copies, waits for them, and re-layouts  5.21 us (3%)
  other arithmetic  4.21 us (3%)
    ppermute x13, starting transfers between devices, from_offset(): lax.ppermute(x, axis, [((i + offset) % count, i) for i in range(count)])  58.3 us
    all_gather x1, blocking collectives, layer(): own = lax.all_gather(piece, Z, axis=0)  34.2 us
    ppermute x13, waiting for transfers between devices, from_offset(): lax.ppermute(x, axis, [((i + offset) % count, i) for i in range(count)])  31.7 us
    pallas_call x1, Pallas kernels, project(): pl.pallas_call(project_kernel, out_shape=(jax.ShapeDtypeStruct((rows, 384...  6.02 us
    unnamed x16, local copies, waits for them, and re-layouts  4.06 us
    pallas_call x1, Pallas kernels, inner(): pl.pallas_call(inner_kernel, out_shape=(jax.ShapeDtypeStruct((256, 256),...  3.83 us
    pallas_call x1, Pallas kernels, outer(): pl.pallas_call(outer_kernel, out_shape=(jax.ShapeDtypeStruct((128, 2048),...  3.7 us
    ppermute x1, starting transfers between devices, halo(): low = lax.ppermute(block[-width:], SP, forward)  3.61 us
  transfers between devices with their start and end apart: 15, of which 4 were waited for; matrix products, arithmetic and copies ran while one was open for 1% of the time, Pallas kernels for 4%

profile of v1, /device:TPU:1, one launch (start us, length us, event | category | flops | bytes accessed | tf_op | source)
XLA Modules:
  0.0 160.6 jit_solution(9600880648918651712)
XLA Ops:
  0.6 0.9 concatenate.6
  1.5 34.2 %all-gather = bf16[256,1664]{1,0:T(8,128)(2,1)S(1)} all-gather(bf16[16,1664]{1,0:T(8,128)(2,1)S(1)} %concatenate.6), channel_id=2, replica_groups=mesh['sp_0'=16,'sp_1'=4,'sp_2'=2,'tp'=4] {'sp_0'}, dimensions={0}, use_global_device_ids=true | all-gather | bytes 905216 | tf_op jit(solution)/shard_map/all_gather | solution.py:354
  35.7 3.1 %collective-permute-start.5 = (bf16[16,16,1664]{2,1,0:T(8,128)(2,1)S(1)}, bf16[16,16,1664]{2,1,0:T(8,128)(2,1)S(1)}, u32[]{:S(2)}, u32[]{:S(2)}) collective-permute-start(bf16[16,16,1664]{2,1,0:T(8,128)(2,1)S(1)} %bitcast.6), channel_id=1, source_target_pairs={{24,0},{0,8},{8,16},{16,24},{25,1},{1,9},{9,17},{17,25},{26,2},{2,... | collective-permute-start | bytes 2555912 | tf_op jit(solution)/shard_map/ppermute | solution.py:33
  38.8 4.4 %collective-permute-start.4 = (bf16[16,16,1664]{2,1,0:T(8,128)(2,1)S(1)}, bf16[16,16,1664]{2,1,0:T(8,128)(2,1)S(1)}, u32[]{:S(2)}, u32[]{:S(2)}) collective-permute-start(bf16[16,16,1664]{2,1,0:T(8,128)(2,1)S(1)} %bitcast.7), channel_id=1, source_target_pairs={{16,0},{24,8},{0,16},{8,24},{17,1},{25,9},{1,17},{9,25},{18,2},{26... | collective-permute-start | bytes 2555912 | tf_op jit(solution)/shard_map/ppermute | solution.py:33
  43.2 3.1 %collective-permute-start.3 = (bf16[16,16,1664]{2,1,0:T(8,128)(2,1)S(1)}, bf16[16,16,1664]{2,1,0:T(8,128)(2,1)}, u32[]{:S(2)}, u32[]{:S(2)}) collective-permute-start(bf16[16,16,1664]{2,1,0:T(8,128)(2,1)S(1)} %bitcast.8), channel_id=1, source_target_pairs={{8,0},{16,8},{24,16},{0,24},{9,1},{17,9},{25,17},{1,25},{10,2},{18... | collective-permute-start | bytes 2555912 | tf_op jit(solution)/shard_map/ppermute | solution.py:33
  46.3 3.2 %collective-permute-start.2 = (bf16[512,512]{1,0:T(8,128)(2,1)}, bf16[512,512]{1,0:T(8,128)(2,1)S(1)}, u32[]{:S(2)}, u32[]{:S(2)}) collective-permute-start(bf16[512,512]{1,0:T(8,128)(2,1)} %refs_0_.1), channel_id=1, source_target_pairs={{3,0},{0,1},{1,2},{2,3},{7,4},{4,5},{5,6},{6,7},{11,8},{8,9},{9,10... | collective-permute-start | bytes 1572872 | tf_op jit(solution)/shard_map/ppermute | solution.py:33
  49.5 4.5 %collective-permute-start.1 = (bf16[512,512]{1,0:T(8,128)(2,1)}, bf16[512,512]{1,0:T(8,128)(2,1)}, u32[]{:S(2)}, u32[]{:S(2)}) collective-permute-start(bf16[512,512]{1,0:T(8,128)(2,1)} %refs_0_.1), channel_id=1, source_target_pairs={{2,0},{3,1},{0,2},{1,3},{6,4},{7,5},{4,6},{5,7},{10,8},{11,9},{8,1... | collective-permute-start | bytes 1572872 | tf_op jit(solution)/shard_map/ppermute | solution.py:33
  54.0 3.9 %collective-permute-done.2.refs_3_ = bf16[512,512]{1,0:T(8,128)(2,1)S(1)} collective-permute-done((bf16[512,512]{1,0:T(8,128)(2,1)}, bf16[512,512]{1,0:T(8,128)(2,1)S(1)}, u32[]{:S(2)}, u32[]{:S(2)}) %collective-permute-start.2) | collective-permute-done | bytes 524320 | tf_op jit(solution)/shard_map/ppermute | solution.py:33
  58.0 14.7 %collective-permute-start.6 = (bf16[16,16,1664]{2,1,0:T(8,128)(2,1)S(1)}, bf16[16,16,1664]{2,1,0:T(8,128)(2,1)}, u32[]{:S(2)}, u32[]{:S(2)}) collective-permute-start(bf16[16,16,1664]{2,1,0:T(8,128)(2,1)S(1)} %bitcast.9), channel_id=1, source_target_pairs={{4,0},{0,4},{5,1},{1,5},{6,2},{2,6},{7,3},{3,7},{12,8},{8,12},{13,... | collective-permute-start | bytes 2555912 | tf_op jit(solution)/shard_map/ppermute | solution.py:33
  72.7 1.9 %collective-permute-start.9 = (bf16[16,16,1664]{2,1,0:T(8,128)(2,1)S(1)}, bf16[16,16,1664]{2,1,0:T(8,128)(2,1)}, u32[]{:S(2)}, u32[]{:S(2)}) collective-permute-start(bf16[16,16,1664]{2,1,0:T(8,128)(2,1)S(1)} %collective-permute-done.5.refs_6_.refs_3_), channel_id=1, source_target_pairs={{4,0},{0,4},{5,1},{1,5},{6,2},{2,6},{7,3},{3,7},{12,8},{8,12},{13,... | collective-permute-start | bytes 2555912 | tf_op jit(solution)/shard_map/ppermute | solution.py:33
  74.7 6.7 %collective-permute-start.8 = (bf16[16,16,1664]{2,1,0:T(8,128)(2,1)S(1)}, bf16[16,16,1664]{2,1,0:T(8,128)(2,1)}, u32[]{:S(2)}, u32[]{:S(2)}) collective-permute-start(bf16[16,16,1664]{2,1,0:T(8,128)(2,1)S(1)} %collective-permute-done.4.refs_5_.refs_2_), channel_id=1, source_target_pairs={{4,0},{0,4},{5,1},{1,5},{6,2},{2,6},{7,3},{3,7},{12,8},{8,12},{13,... | collective-permute-start | bytes 2555912 | tf_op jit(solution)/shard_map/ppermute | solution.py:33
  81.3 1.9 %collective-permute-start.7 = (bf16[16,16,1664]{2,1,0:T(8,128)(2,1)}, bf16[16,16,1664]{2,1,0:T(8,128)(2,1)}, u32[]{:S(2)}, u32[]{:S(2)}) collective-permute-start(bf16[16,16,1664]{2,1,0:T(8,128)(2,1)} %collective-permute-done.3.refs_4_.refs_1_), channel_id=1, source_target_pairs={{4,0},{0,4},{5,1},{1,5},{6,2},{2,6},{7,3},{3,7},{12,8},{8,12},{13,... | collective-permute-start | bytes 2555912 | tf_op jit(solution)/shard_map/ppermute | solution.py:33
  83.3 4.6 %collective-permute-start = (bf16[512,512]{1,0:T(8,128)(2,1)}, bf16[512,512]{1,0:T(8,128)(2,1)S(1)}, u32[]{:S(2)}, u32[]{:S(2)}) collective-permute-start(bf16[512,512]{1,0:T(8,128)(2,1)} %refs_0_.1), channel_id=1, source_target_pairs={{1,0},{2,1},{3,2},{0,3},{5,4},{6,5},{7,6},{4,7},{9,8},{10,9},{11,1... | collective-permute-start | bytes 1572872 | tf_op jit(solution)/shard_map/ppermute | solution.py:33
  88.0 1.1 negate_select_fusion
  89.1 10.0 %collective-permute-done.refs_1_ = bf16[512,512]{1,0:T(8,128)(2,1)S(1)} collective-permute-done((bf16[512,512]{1,0:T(8,128)(2,1)}, bf16[512,512]{1,0:T(8,128)(2,1)S(1)}, u32[]{:S(2)}, u32[]{:S(2)}) %collective-permute-start) | collective-permute-done | bytes 524320 | tf_op jit(solution)/shard_map/ppermute | solution.py:33
  99.1 1.0 copy-done.4
  100.8 2.5 %shard_map.131.refs_0_ = bf16[512,2048]{1,0:T(8,128)(2,1)S(1)} custom-call(f32[1,2048]{1,0:T(1,128)S(1)} %bitcast.12, bf16[512,512]{1,0:T(8,128)(2,1)S(1)} %copy-done.4, bf16[512,512]{1,0:T(8,128)(2,1)S(1)} %collective-permute-done.refs_1_, bf16[512,512]{1,0:T(8,128)(2,1)} %collective-permute-done.1.refs_2_, bf16[512,512]{1,0:T(8,128)(2,1)S(1)} %collective-permute-done.2.refs_3_), custom_call_target="tpu_custom_call" | custom-call | flops 500000000 | bytes 4000000 | tf_op jit(solution)/shard_map/pallas_call | solution.py:70
  103.3 6.0 %shard_map.132 = (bf16[512,384]{1,0:T(8,128)(2,1)S(1)}, bf16[512,256]{1,0:T(8,128)(2,1)S(1)}, f32[512,256]{1,0:T(8,128)S(1)}) custom-call(bf16[512,2048]{1,0:T(8,128)(2,1)S(1)} %shard_map.131.refs_0_, f32[512,128]{1,0:T(8,128)S(1)} %get-tuple-element.35.refs_1_, f32[512,128]{1,0:T(8,128)S(1)} %get-tuple-element.34.refs_2_, ...), custom_call_target="tpu_custom_call" | custom-call | flops 2415919104 | bytes 8000000 | tf_op jit(solution)/shard_map/pallas_call | solution.py:129
  109.4 3.3 %collective-permute-start.11 = (bf16[128,384]{1,0:T(8,128)(2,1)S(1)}, bf16[128,384]{1,0:T(8,128)(2,1)S(1)}, u32[]{:S(2)}, u32[]{:S(2)}) collective-permute-start(bf16[128,384]{1,0:T(8,128)(2,1)S(1)} %get-tuple-element.30), channel_id=1, source_target_pairs={{4,0},{8,4},{12,8},{16,12},{20,16},{24,20},{28,24},{32,28},{36,32}... | collective-permute-start | bytes 294920 | tf_op jit(solution)/shard_map/ppermute | solution.py:310
  112.7 3.6 %collective-permute-start.10 = (bf16[128,384]{1,0:T(8,128)(2,1)S(1)}, bf16[128,384]{1,0:T(8,128)(2,1)S(1)}, u32[]{:S(2)}, u32[]{:S(2)}) collective-permute-start(bf16[128,384]{1,0:T(8,128)(2,1)S(1)} %get-tuple-element.31), channel_id=1, source_target_pairs={{0,4},{4,8},{8,12},{12,16},{16,20},{20,24},{24,28},{28,32},{32,36}... | collective-permute-start | bytes 294920 | tf_op jit(solution)/shard_map/ppermute | solution.py:309
  116.3 1.1 copy-done.1
  117.4 1.2 copy-done.3
  118.6 3.8 %shard_map.133 = (bf16[256,256]{1,0:T(8,128)(2,1)S(1)}, f32[256,4]{1,0:T(8,128)S(1)}, bf16[2048,512]{1,0:T(8,128)(2,1)S(1)}) custom-call(f32[4]{0:T(128)S(1)} %copy-done.6, bf16[512,256]{1,0:T(8,128)(2,1)S(1)} %get-tuple-element.17.query_ref, bf16[512,384]{1,0:T(8,128)(2,1)S(1)} %get-tuple-element.18.kvc_ref, bf16[16,16,1664]{2,1,0:T(8,128)(2,1)S(1)} %bitcast.11, ...), custom_call_target="tpu_custom_call" | custom-call | flops 2013265920 | bytes 2000000 | tf_op jit(solution)/shard_map/pallas_call | solution.py:205
  122.5 3.7 %shard_map.134 = (bf16[128,2048]{1,0:T(8,128)(2,1)}, bf16[512,512]{1,0:T(8,128)(2,1)S(1)}, f32[256,4]{1,0:T(8,128)S(1)}) custom-call(f32[4]{0:T(128)S(1)} %copy-done.6, bf16[512,256]{1,0:T(8,128)(2,1)S(1)} %get-tuple-element.17.query_ref, bf16[512,384]{1,0:T(8,128)(2,1)S(1)} %get-tuple-element.18.kvc_ref, ...), custom_call_target="tpu_custom_call" | custom-call | flops 1073741824 | bytes 8000000 | tf_op jit(solution)/shard_map/pallas_call | solution.py:289
  126.2 2.3 %shard_map.136 = (bf16[128,2048]{1,0:T(8,128)(2,1)}, bf16[128,2048]{1,0:T(8,128)(2,1)}) custom-call(bf16[512,512]{1,0:T(8,128)(2,1)S(1)} %get-tuple-element.22.both_ref, bf16[2048,512]{1,0:T(8,128)(2,1)S(1)} %get-tuple-element.21.out_rows_ref), custom_call_target="tpu_custom_call" | custom-call | flops 536870912 | bytes 3000000 | tf_op jit(solution)/shard_map/pallas_call | solution.py:276
  128.4 2.6 %collective-permute-start.13 = (bf16[128,2048]{1,0:T(8,128)(2,1)}, bf16[128,2048]{1,0:T(8,128)(2,1)}, u32[]{:S(2)}, u32[]{:S(2)}) collective-permute-start(bf16[128,2048]{1,0:T(8,128)(2,1)} %get-tuple-element.24), channel_id=1, source_target_pairs={{3,0},{0,1},{1,2},{2,3},{7,4},{4,5},{5,6},{6,7},{11,8},{8,9},{9,10... | collective-permute-start | bytes 1572872 | tf_op jit(solution)/shard_map/ppermute | solution.py:33
  131.0 4.5 %collective-permute-start.14 = (bf16[128,2048]{1,0:T(8,128)(2,1)}, bf16[128,2048]{1,0:T(8,128)(2,1)}, u32[]{:S(2)}, u32[]{:S(2)}) collective-permute-start(bf16[128,2048]{1,0:T(8,128)(2,1)} %get-tuple-element.25), channel_id=1, source_target_pairs={{1,0},{2,1},{3,2},{0,3},{5,4},{6,5},{7,6},{4,7},{9,8},{10,9},{11,1... | collective-permute-start | bytes 1572872 | tf_op jit(solution)/shard_map/ppermute | solution.py:33
  135.6 3.1 %collective-permute-start.12 = (bf16[128,2048]{1,0:T(8,128)(2,1)}, bf16[128,2048]{1,0:T(8,128)(2,1)}, u32[]{:S(2)}, u32[]{:S(2)}) collective-permute-start(bf16[128,2048]{1,0:T(8,128)(2,1)} %get-tuple-element.23), channel_id=1, source_target_pairs={{2,0},{3,1},{0,2},{1,3},{6,4},{7,5},{4,6},{5,7},{10,8},{11,9},{8,1... | collective-permute-start | bytes 1572872 | tf_op jit(solution)/shard_map/ppermute | solution.py:33
  138.9 0.8 shard_map.135
  140.4 4.8 %collective-permute-done.13 = bf16[128,2048]{1,0:T(8,128)(2,1)} collective-permute-done((bf16[128,2048]{1,0:T(8,128)(2,1)}, bf16[128,2048]{1,0:T(8,128)(2,1)}, u32[]{:S(2)}, u32[]{:S(2)}) %collective-permute-start.13) | collective-permute-done | bytes 524320 | tf_op jit(solution)/shard_map/ppermute | solution.py:33
  145.1 13.0 %collective-permute-done.14 = bf16[128,2048]{1,0:T(8,128)(2,1)} collective-permute-done((bf16[128,2048]{1,0:T(8,128)(2,1)}, bf16[128,2048]{1,0:T(8,128)(2,1)}, u32[]{:S(2)}, u32[]{:S(2)}) %collective-permute-start.14) | collective-permute-done | bytes 524320 | tf_op jit(solution)/shard_map/ppermute | solution.py:33
  158.2 2.5 %add_convert_fusion = bf16[128,2048]{1,0:T(8,128)(2,1)} fusion(bf16[128,2048]{1,0:T(8,128)(2,1)} %collective-permute-done.14, bf16[128,2048]{1,0:T(8,128)(2,1)} %collective-permute-done.13, bf16[128,2048]{1,0:T(8,128)(2,1)} %collective-permute-done.12, bf16[128,2048]{1,0:T(8,128)(2,1)S(1)} %shard_map.135), kind=kLoop, calls=%fused_computation | loop fusion | flops 2097152 | bytes 2621440 | tf_op jit(solution)/shard_map/convert_element_type | solution.py:374
  (38 shorter events, 1.7 us)
Async XLA Ops:
  35.7 37.0 %collective-permute-start.5 = (bf16[16,16,1664]{2,1,0:T(8,128)(2,1)S(1)}, bf16[16,16,1664]{2,1,0:T(8,128)(2,1)S(1)}, u32[]{:S(2)}, u32[]{:S(2)}) collective-permute-start(bf16[16,16,1664]{2,1,0:T(8,128)(2,1)S(1)} %bitcast.6), channel_id=1, source_target_pairs={{24,0},{0,8},{8,16},{16,24},{25,1},{1,9},{9,17},{17,25},{26,2},{2,... | collective-permute-start | bytes 2555912 | tf_op jit(solution)/shard_map/ppermute | solution.py:33
  38.8 35.8 %collective-permute-start.4 = (bf16[16,16,1664]{2,1,0:T(8,128)(2,1)S(1)}, bf16[16,16,1664]{2,1,0:T(8,128)(2,1)S(1)}, u32[]{:S(2)}, u32[]{:S(2)}) collective-permute-start(bf16[16,16,1664]{2,1,0:T(8,128)(2,1)S(1)} %bitcast.7), channel_id=1, source_target_pairs={{16,0},{24,8},{0,16},{8,24},{17,1},{25,9},{1,17},{9,25},{18,2},{26... | collective-permute-start | bytes 2555912 | tf_op jit(solution)/shard_map/ppermute | solution.py:33
  43.2 38.1 %collective-permute-start.3 = (bf16[16,16,1664]{2,1,0:T(8,128)(2,1)S(1)}, bf16[16,16,1664]{2,1,0:T(8,128)(2,1)}, u32[]{:S(2)}, u32[]{:S(2)}) collective-permute-start(bf16[16,16,1664]{2,1,0:T(8,128)(2,1)S(1)} %bitcast.8), channel_id=1, source_target_pairs={{8,0},{16,8},{24,16},{0,24},{9,1},{17,9},{25,17},{1,25},{10,2},{18... | collective-permute-start | bytes 2555912 | tf_op jit(solution)/shard_map/ppermute | solution.py:33
  46.3 11.7 %collective-permute-start.2 = (bf16[512,512]{1,0:T(8,128)(2,1)}, bf16[512,512]{1,0:T(8,128)(2,1)S(1)}, u32[]{:S(2)}, u32[]{:S(2)}) collective-permute-start(bf16[512,512]{1,0:T(8,128)(2,1)} %refs_0_.1), channel_id=1, source_target_pairs={{3,0},{0,1},{1,2},{2,3},{7,4},{4,5},{5,6},{6,7},{11,8},{8,9},{9,10... | collective-permute-start | bytes 1572872 | tf_op jit(solution)/shard_map/ppermute | solution.py:33
  49.5 33.8 %collective-permute-start.1 = (bf16[512,512]{1,0:T(8,128)(2,1)}, bf16[512,512]{1,0:T(8,128)(2,1)}, u32[]{:S(2)}, u32[]{:S(2)}) collective-permute-start(bf16[512,512]{1,0:T(8,128)(2,1)} %refs_0_.1), channel_id=1, source_target_pairs={{2,0},{3,1},{0,2},{1,3},{6,4},{7,5},{4,6},{5,7},{10,8},{11,9},{8,1... | collective-permute-start | bytes 1572872 | tf_op jit(solution)/shard_map/ppermute | solution.py:33
  58.0 45.3 %collective-permute-start.6 = (bf16[16,16,1664]{2,1,0:T(8,128)(2,1)S(1)}, bf16[16,16,1664]{2,1,0:T(8,128)(2,1)}, u32[]{:S(2)}, u32[]{:S(2)}) collective-permute-start(bf16[16,16,1664]{2,1,0:T(8,128)(2,1)S(1)} %bitcast.9), channel_id=1, source_target_pairs={{4,0},{0,4},{5,1},{1,5},{6,2},{2,6},{7,3},{3,7},{12,8},{8,12},{13,... | collective-permute-start | bytes 2555912 | tf_op jit(solution)/shard_map/ppermute | solution.py:33
  72.7 30.6 %copy-start = (bf16[16,16,1664]{2,1,0:T(8,128)(2,1)}, bf16[16,16,1664]{2,1,0:T(8,128)(2,1)S(1)}, u32[]{:S(2)}) copy-start(bf16[16,16,1664]{2,1,0:T(8,128)(2,1)S(1)} %collective-permute-done.5.refs_6_.refs_3_) | copy-start | bytes 2555908
  72.7 30.6 %collective-permute-start.9 = (bf16[16,16,1664]{2,1,0:T(8,128)(2,1)S(1)}, bf16[16,16,1664]{2,1,0:T(8,128)(2,1)}, u32[]{:S(2)}, u32[]{:S(2)}) collective-permute-start(bf16[16,16,1664]{2,1,0:T(8,128)(2,1)S(1)} %collective-permute-done.5.refs_6_.refs_3_), channel_id=1, source_target_pairs={{4,0},{0,4},{5,1},{1,5},{6,2},{2,6},{7,3},{3,7},{12,8},{8,12},{13,... | collective-permute-start | bytes 2555912 | tf_op jit(solution)/shard_map/ppermute | solution.py:33
  74.6 28.7 %copy-start.2 = (bf16[16,16,1664]{2,1,0:T(8,128)(2,1)}, bf16[16,16,1664]{2,1,0:T(8,128)(2,1)S(1)}, u32[]{:S(2)}) copy-start(bf16[16,16,1664]{2,1,0:T(8,128)(2,1)S(1)} %collective-permute-done.4.refs_5_.refs_2_) | copy-start | bytes 2555908
  74.7 28.6 %collective-permute-start.8 = (bf16[16,16,1664]{2,1,0:T(8,128)(2,1)S(1)}, bf16[16,16,1664]{2,1,0:T(8,128)(2,1)}, u32[]{:S(2)}, u32[]{:S(2)}) collective-permute-start(bf16[16,16,1664]{2,1,0:T(8,128)(2,1)S(1)} %collective-permute-done.4.refs_5_.refs_2_), channel_id=1, source_target_pairs={{4,0},{0,4},{5,1},{1,5},{6,2},{2,6},{7,3},{3,7},{12,8},{8,12},{13,... | collective-permute-start | bytes 2555912 | tf_op jit(solution)/shard_map/ppermute | solution.py:33
  81.3 22.0 %collective-permute-start.7 = (bf16[16,16,1664]{2,1,0:T(8,128)(2,1)}, bf16[16,16,1664]{2,1,0:T(8,128)(2,1)}, u32[]{:S(2)}, u32[]{:S(2)}) collective-permute-start(bf16[16,16,1664]{2,1,0:T(8,128)(2,1)} %collective-permute-done.3.refs_4_.refs_1_), channel_id=1, source_target_pairs={{4,0},{0,4},{5,1},{1,5},{6,2},{2,6},{7,3},{3,7},{12,8},{8,12},{13,... | collective-permute-start | bytes 2555912 | tf_op jit(solution)/shard_map/ppermute | solution.py:33
  83.3 15.7 %collective-permute-start = (bf16[512,512]{1,0:T(8,128)(2,1)}, bf16[512,512]{1,0:T(8,128)(2,1)S(1)}, u32[]{:S(2)}, u32[]{:S(2)}) collective-permute-start(bf16[512,512]{1,0:T(8,128)(2,1)} %refs_0_.1), channel_id=1, source_target_pairs={{1,0},{2,1},{3,2},{0,3},{5,4},{6,5},{7,6},{4,7},{9,8},{10,9},{11,1... | collective-permute-start | bytes 1572872 | tf_op jit(solution)/shard_map/ppermute | solution.py:33
  99.0 1.0 copy-start.4
  100.1 0.7 copy-start.5
  103.3 13.0 %copy-start.6 = (f32[4]{0:T(128)S(1)}, f32[4]{0:T(128)}, u32[]{:S(2)}) copy-start(f32[4]{0:T(128)} %sink_ref.3) | copy-start | bytes 52
  109.4 13.1 %collective-permute-start.11 = (bf16[128,384]{1,0:T(8,128)(2,1)S(1)}, bf16[128,384]{1,0:T(8,128)(2,1)S(1)}, u32[]{:S(2)}, u32[]{:S(2)}) collective-permute-start(bf16[128,384]{1,0:T(8,128)(2,1)S(1)} %get-tuple-element.30), channel_id=1, source_target_pairs={{4,0},{8,4},{12,8},{16,12},{20,16},{24,20},{28,24},{32,28},{36,32}... | collective-permute-start | bytes 294920 | tf_op jit(solution)/shard_map/ppermute | solution.py:310
  112.7 9.8 %collective-permute-start.10 = (bf16[128,384]{1,0:T(8,128)(2,1)S(1)}, bf16[128,384]{1,0:T(8,128)(2,1)S(1)}, u32[]{:S(2)}, u32[]{:S(2)}) collective-permute-start(bf16[128,384]{1,0:T(8,128)(2,1)S(1)} %get-tuple-element.31), channel_id=1, source_target_pairs={{0,4},{4,8},{8,12},{12,16},{16,20},{20,24},{24,28},{28,32},{32,36}... | collective-permute-start | bytes 294920 | tf_op jit(solution)/shard_map/ppermute | solution.py:309
  116.3 1.2 copy-start.1
  117.4 1.2 copy-start.3
  118.6 3.9 %copy-start.7 = (f32[3,256]{1,0:T(4,128)S(1)}, f32[3,256]{1,0:T(4,128)}, u32[]{:S(2)}) copy-start(f32[3,256]{1,0:T(4,128)} %taps_ref.1) | copy-start | bytes 9220
  128.4 16.7 %collective-permute-start.13 = (bf16[128,2048]{1,0:T(8,128)(2,1)}, bf16[128,2048]{1,0:T(8,128)(2,1)}, u32[]{:S(2)}, u32[]{:S(2)}) collective-permute-start(bf16[128,2048]{1,0:T(8,128)(2,1)} %get-tuple-element.24), channel_id=1, source_target_pairs={{3,0},{0,1},{1,2},{2,3},{7,4},{4,5},{5,6},{6,7},{11,8},{8,9},{9,10... | collective-permute-start | bytes 1572872 | tf_op jit(solution)/shard_map/ppermute | solution.py:33
  131.0 27.1 %collective-permute-start.14 = (bf16[128,2048]{1,0:T(8,128)(2,1)}, bf16[128,2048]{1,0:T(8,128)(2,1)}, u32[]{:S(2)}, u32[]{:S(2)}) collective-permute-start(bf16[128,2048]{1,0:T(8,128)(2,1)} %get-tuple-element.25), channel_id=1, source_target_pairs={{1,0},{2,1},{3,2},{0,3},{5,4},{6,5},{7,6},{4,7},{9,8},{10,9},{11,1... | collective-permute-start | bytes 1572872 | tf_op jit(solution)/shard_map/ppermute | solution.py:33
  135.6 22.6 %collective-permute-start.12 = (bf16[128,2048]{1,0:T(8,128)(2,1)}, bf16[128,2048]{1,0:T(8,128)(2,1)}, u32[]{:S(2)}, u32[]{:S(2)}) collective-permute-start(bf16[128,2048]{1,0:T(8,128)(2,1)} %get-tuple-element.23), channel_id=1, source_target_pairs={{2,0},{3,1},{0,2},{1,3},{6,4},{7,5},{4,6},{5,7},{10,8},{11,9},{8,1... | collective-permute-start | bytes 1572872 | tf_op jit(solution)/shard_map/ppermute | solution.py:33

commit v2 on v1

--- a/solution.py
+++ b/solution.py
@@ -41,7 +41,7 @@
     far, up, down = (from_offset(own, X, step) for step in (2, 1, 3))
     mine = (own, up, far, down)
     swapped = []
-    for part in mine:
+    for part in (own, up, far, down):
         swapped.append(from_offset(part, CORE, 1))
     return (*mine, *swapped)
 
@@ -100,8 +100,9 @@
 
 def project_kernel(*refs):
     normed_ref, cos_ref, sin_ref = refs[:3]
-    kvc_ref, query_ref, post_ref, rows_ref = refs[11:]
+    kvc_ref, query_ref, post_ref, out_rows_ref, rows_ref = refs[11:]
     place_rows(refs[3:11], rows_ref, slice(0, 1152))
+    place_rows(refs[3:11], out_rows_ref, slice(1152, 1664))
 
     def projected(first, last):
         return jnp.dot(
@@ -132,9 +133,10 @@
             jax.ShapeDtypeStruct((rows, 384), jnp.bfloat16),
             jax.ShapeDtypeStruct((rows, 256), jnp.bfloat16),
             jax.ShapeDtypeStruct((rows, 256), jnp.float32),
+            jax.ShapeDtypeStruct((2048, 512), jnp.bfloat16),
         ),
         in_specs=[VMEM] * 11,
-        out_specs=(VMEM,) * 3,
+        out_specs=(VMEM,) * 4,
         scratch_shapes=[pltpu.VMEM((2048, 1152), jnp.bfloat16)],
         compiler_params=params(24),
         cost_estimate=pl.CostEstimate(
@@ -183,9 +185,7 @@
     return lax.axis_index(SP) * 512
 
 
-def inner_kernel(sink_ref, query_ref, kvc_ref, *refs):
-    attended_ref, log_ref, out_rows_ref = refs[8:]
-    place_rows(refs[:8], out_rows_ref, slice(1152, 1664))
+def inner_kernel(sink_ref, query_ref, kvc_ref, attended_ref, log_ref):
     sinks = [sink_ref[h] for h in range(4)]
     bias = window_bias()
     for n in (1, 2):
@@ -201,21 +201,20 @@
         log_ref[(n - 1) * WINDOW : n * WINDOW, :] = log_sum
 
 
-def inner(sinks, query, kvc, parts):
+def inner(sinks, query, kvc):
     return pl.pallas_call(
         inner_kernel,
         out_shape=(
             jax.ShapeDtypeStruct((256, 256), jnp.bfloat16),
             jax.ShapeDtypeStruct((256, 4), jnp.float32),
-            jax.ShapeDtypeStruct((2048, 512), jnp.bfloat16),
-        ),
-        in_specs=[SMEM] + [VMEM] * 10,
-        out_specs=(VMEM,) * 3,
+        ),
+        in_specs=[SMEM, VMEM, VMEM],
+        out_specs=(VMEM, VMEM),
         compiler_params=params(12),
         cost_estimate=pl.CostEstimate(
             flops=2 * 2 * 1024 * 384 * 64 * 20, bytes_accessed=2_000_000, transcendentals=400_000
         ),
-    )(sinks, query, kvc, *parts)
+    )(sinks, query, kvc)
 
 
 def outer_kernel(
@@ -250,46 +249,54 @@
     following = jnp.where(row == rows - 1, after, pltpu.roll(conv, rows - 1, 0))
     convolved = taps_ref[0:1] * previous + taps_ref[1:2] * conv + taps_ref[2:3] * following
     both_ref[:, 256:] = (post_ref[...] * convolved).astype(jnp.bfloat16)
-    send_chunk(both_ref, out_rows_ref, far_ref, 2)
-
-
-def send_chunk(both_ref, out_rows_ref, out_ref, step):
+    far = chunk(both_ref, out_rows_ref, 2).astype(jnp.bfloat16)
+    half = far.shape[1] // 2
+    far_ref[0] = far[:, :half]
+    far_ref[1] = far[:, half:]
+
+
+def chunk(both_ref, out_rows_ref, step):
     block = lax.rem(lax.axis_index("tp") + step, 4)
-    out_ref[...] = lax.dot_general(
+    return lax.dot_general(
         both_ref[pl.ds(pl.multiple_of(block * WINDOW, WINDOW), WINDOW), :],
         out_rows_ref[...],
         (((1,), (1,)), ((), ())),
         preferred_element_type=jnp.float32,
-    ).astype(jnp.bfloat16)
-
-
-def near_kernel(both_ref, out_rows_ref, up_ref, down_ref):
-    send_chunk(both_ref, out_rows_ref, up_ref, 1)
-    send_chunk(both_ref, out_rows_ref, down_ref, 3)
+    )
+
+
+def near_kernel(both_ref, out_rows_ref, low_ref, high_ref, up_ref, down_ref):
+    half = low_ref.shape[1]
+    up = chunk(both_ref, out_rows_ref, 1)
+    up_ref[:, :half] = (up[:, :half] + low_ref[...].astype(jnp.float32)).astype(jnp.bfloat16)
+    up_ref[:, half:] = up[:, half:].astype(jnp.bfloat16)
+    down = chunk(both_ref, out_rows_ref, 3)
+    down_ref[:, :half] = down[:, :half].astype(jnp.bfloat16)
+    down_ref[:, half:] = (down[:, half:] + high_ref[...].astype(jnp.float32)).astype(jnp.bfloat16)
 
 
 def own_kernel(both_ref, out_rows_ref, own_ref):
-    send_chunk(both_ref, out_rows_ref, own_ref, 0)
-
-
-def chunks(kernel, count, both, out_rows):
+    own_ref[...] = chunk(both_ref, out_rows_ref, 0).astype(jnp.bfloat16)
+
+
+def chunks(kernel, count, *arrays):
     return pl.pallas_call(
         kernel,
         out_shape=(jax.ShapeDtypeStruct((128, 2048), jnp.bfloat16),) * count,
-        in_specs=[VMEM] * 2,
+        in_specs=[VMEM] * len(arrays),
         out_specs=(VMEM,) * count,
         compiler_params=params(12),
         cost_estimate=pl.CostEstimate(
             flops=count * 2 * 128 * 512 * 2048, bytes_accessed=3_000_000, transcendentals=0
         ),
-    )(both, out_rows)
+    )(*arrays)
 
 
 def outer(sinks, query, kvc, low, high, post, taps, inner_attended, out_rows):
     return pl.pallas_call(
         outer_kernel,
         out_shape=(
-            jax.ShapeDtypeStruct((128, 2048), jnp.bfloat16),
+            jax.ShapeDtypeStruct((2, 128, 1024), jnp.bfloat16),
             jax.ShapeDtypeStruct((512, 512), jnp.bfloat16),
             jax.ShapeDtypeStruct((256, 4), jnp.float32),
         ),
@@ -351,21 +358,22 @@
         ],
         axis=1,
     )
-    own = lax.all_gather(piece, Z, axis=0)
     cosine, sine = rotation_tables(rows)
+    own = lax.all_gather(after(piece, (cosine, sine)), Z, axis=0)
     parts = gathered_parts(own)
     late_tokens = after(tokens, own)
     arrived = [from_offset(late_tokens, "tp", step) for step in (1, 2, 3)]
-    normed = normalized(after(norm_gain[None], (cosine, sine)), [tokens, *arrived])
-    kvc, query, post = project(normed, cosine, sine, parts)
+    normed = normalized(norm_gain[None], [tokens, *arrived])
+    kvc, query, post, out_rows = project(normed, cosine, sine, parts)
     low, high = halo(kvc, WINDOW)
-    inner_attended, inner_log, out_rows = inner(sink_logit, query, kvc, parts)
+    inner_attended, inner_log = inner(sink_logit, query, kvc)
     far, both, outer_log = outer(
         sink_logit, query, kvc, low, high, post, conv_taps, inner_attended, out_rows
     )
-    arrived = [from_offset(far, "tp", -2)]
-    up, down = chunks(near_kernel, 2, both, out_rows)
-    arrived += [from_offset(up, "tp", -1), from_offset(down, "tp", -3)]
+    low_half = from_offset(far[0], "tp", -1)
+    high_half = from_offset(far[1], "tp", 1)
+    up, down = chunks(near_kernel, 2, both, out_rows, low_half, high_half)
+    arrived = [from_offset(up, "tp", -1), from_offset(down, "tp", 1)]
     (mine,) = chunks(own_kernel, 1, both, out_rows)
     total = mine.astype(jnp.float32)
     for block in arrived:

time: 162 us -> 159 us (0.981)
  Pallas kernels: 19.1 us -> 12.8 us
  starting transfers between devices: 65.2 us -> 68.5 us
  local copies, waits for them, and re-layouts: 5.21 us -> 2.94 us
    ppermute x13 -> x14, starting transfers between devices: 58.3 us -> 61.7 us  [from_offset(): lax.ppermute(x, axis, [((i + offset) % count, i) for i in range(count)])]
    unnamed x16 -> x8, local copies, waits for them, and re-layouts: 4.06 us -> 1.75 us
    pallas_call x1, Pallas kernels: 6.02 us -> 3.98 us  [project(): pl.pallas_call(project_kernel, out_shape=(jax.ShapeDtypeStruct((rows, 384...]
    pallas_call x1, Pallas kernels: 3.83 us -> 2.08 us  [inner(): pl.pallas_call(inner_kernel, out_shape=(jax.ShapeDtypeStruct((256, 256),...]
    ppermute x13 -> x14, waiting for transfers between devices: 31.7 us -> 32.9 us  [from_offset(): lax.ppermute(x, axis, [((i + offset) % count, i) for i in range(count)])]
  transfers between devices with their start and end apart: 15 -> 16, of which waited for: 4 -> 6; matrix products, arithmetic and copies ran while one was open for 1% -> 1% of each run, Pallas kernels for 4% -> 3%
where the time goes in v2:
time: 159 us; the launch traced here: 156 us
  starting transfers between devices  68.5 us (43%)
  blocking collectives  34.2 us (22%)
  waiting for transfers between devices  32.9 us (21%)
  Pallas kernels  12.8 us (8%)
  other arithmetic  3.96 us (2%)
  local copies, waits for them, and re-layouts  2.94 us (2%)
    ppermute x14, starting transfers between devices, from_offset(): lax.ppermute(x, axis, [((i + offset) % count, i) for i in range(count)])  61.7 us
    all_gather x1, blocking collectives, layer(): own = lax.all_gather(after(piece, (cosine, sine)), Z, axis=0)  34.2 us
    ppermute x14, waiting for transfers between devices, from_offset(): lax.ppermute(x, axis, [((i + offset) % count, i) for i in range(count)])  32.9 us
    pallas_call x1, Pallas kernels, project(): pl.pallas_call(project_kernel, out_shape=(jax.ShapeDtypeStruct((rows, 384...  3.98 us
    ppermute x1, starting transfers between devices, halo(): low = lax.ppermute(block[-width:], SP, forward)  3.51 us
    ppermute x1, starting transfers between devices, halo(): high = lax.ppermute(block[:width], SP, backward)  3.27 us
  transfers between devices with their start and end apart: 16, of which 6 were waited for; matrix products, arithmetic and copies ran while one was open for 1% of the time, Pallas kernels for 3%

profile of v2, /device:TPU:1, one launch (start us, length us, event | category | flops | bytes accessed | tf_op | source)
XLA Modules:
  0.0 156.3 jit_solution(13138926122299287213)
XLA Ops:
  0.7 0.9 concatenate.6
  1.6 1.1 negate_select_fusion
  2.7 34.2 %all-gather = bf16[256,1664]{1,0:T(8,128)(2,1)S(1)} all-gather(bf16[16,1664]{1,0:T(8,128)(2,1)S(1)} %concatenate.6), channel_id=2, replica_groups=mesh['sp_0'=16,'sp_1'=4,'sp_2'=2,'tp'=4] {'sp_0'}, dimensions={0}, use_global_device_ids=true | all-gather | bytes 905216 | tf_op jit(solution)/shard_map/all_gather | solution.py:362
  36.9 3.1 %collective-permute-start.5 = (bf16[16,16,1664]{2,1,0:T(8,128)(2,1)S(1)}, bf16[16,16,1664]{2,1,0:T(8,128)(2,1)S(1)}, u32[]{:S(2)}, u32[]{:S(2)}) collective-permute-start(bf16[16,16,1664]{2,1,0:T(8,128)(2,1)S(1)} %bitcast.10), channel_id=1, source_target_pairs={{24,0},{0,8},{8,16},{16,24},{25,1},{1,9},{9,17},{17,25},{26,2},{2,... | collective-permute-start | bytes 2555912 | tf_op jit(solution)/shard_map/ppermute | solution.py:33
  40.0 4.4 %collective-permute-start.4 = (bf16[16,16,1664]{2,1,0:T(8,128)(2,1)S(1)}, bf16[16,16,1664]{2,1,0:T(8,128)(2,1)S(1)}, u32[]{:S(2)}, u32[]{:S(2)}) collective-permute-start(bf16[16,16,1664]{2,1,0:T(8,128)(2,1)S(1)} %bitcast.11), channel_id=1, source_target_pairs={{16,0},{24,8},{0,16},{8,24},{17,1},{25,9},{1,17},{9,25},{18,2},{26... | collective-permute-start | bytes 2555912 | tf_op jit(solution)/shard_map/ppermute | solution.py:33
  44.4 3.1 %collective-permute-start.3 = (bf16[16,16,1664]{2,1,0:T(8,128)(2,1)S(1)}, bf16[16,16,1664]{2,1,0:T(8,128)(2,1)S(1)}, u32[]{:S(2)}, u32[]{:S(2)}) collective-permute-start(bf16[16,16,1664]{2,1,0:T(8,128)(2,1)S(1)} %bitcast.12), channel_id=1, source_target_pairs={{8,0},{16,8},{24,16},{0,24},{9,1},{17,9},{25,17},{1,25},{10,2},{18... | collective-permute-start | bytes 2555912 | tf_op jit(solution)/shard_map/ppermute | solution.py:33
  47.5 3.2 %collective-permute-start.2 = (bf16[512,512]{1,0:T(8,128)(2,1)}, bf16[512,512]{1,0:T(8,128)(2,1)S(1)}, u32[]{:S(2)}, u32[]{:S(2)}) collective-permute-start(bf16[512,512]{1,0:T(8,128)(2,1)} %refs_0_.1), channel_id=1, source_target_pairs={{3,0},{0,1},{1,2},{2,3},{7,4},{4,5},{5,6},{6,7},{11,8},{8,9},{9,10... | collective-permute-start | bytes 1572872 | tf_op jit(solution)/shard_map/ppermute | solution.py:33
  50.7 4.5 %collective-permute-start.1 = (bf16[512,512]{1,0:T(8,128)(2,1)}, bf16[512,512]{1,0:T(8,128)(2,1)S(1)}, u32[]{:S(2)}, u32[]{:S(2)}) collective-permute-start(bf16[512,512]{1,0:T(8,128)(2,1)} %refs_0_.1), channel_id=1, source_target_pairs={{2,0},{3,1},{0,2},{1,3},{6,4},{7,5},{4,6},{5,7},{10,8},{11,9},{8,1... | collective-permute-start | bytes 1572872 | tf_op jit(solution)/shard_map/ppermute | solution.py:33
  55.2 4.0 %collective-permute-done.2.refs_3_ = bf16[512,512]{1,0:T(8,128)(2,1)S(1)} collective-permute-done((bf16[512,512]{1,0:T(8,128)(2,1)}, bf16[512,512]{1,0:T(8,128)(2,1)S(1)}, u32[]{:S(2)}, u32[]{:S(2)}) %collective-permute-start.2) | collective-permute-done | bytes 524320 | tf_op jit(solution)/shard_map/ppermute | solution.py:33
  59.2 14.7 %collective-permute-start.6 = (bf16[16,16,1664]{2,1,0:T(8,128)(2,1)S(1)}, bf16[16,16,1664]{2,1,0:T(8,128)(2,1)S(1)}, u32[]{:S(2)}, u32[]{:S(2)}) collective-permute-start(bf16[16,16,1664]{2,1,0:T(8,128)(2,1)S(1)} %bitcast.13), channel_id=1, source_target_pairs={{4,0},{0,4},{5,1},{1,5},{6,2},{2,6},{7,3},{3,7},{12,8},{8,12},{13,... | collective-permute-start | bytes 2555912 | tf_op jit(solution)/shard_map/ppermute | solution.py:33
  73.9 1.9 %collective-permute-start.9 = (bf16[16,16,1664]{2,1,0:T(8,128)(2,1)S(1)}, bf16[16,16,1664]{2,1,0:T(8,128)(2,1)S(1)}, u32[]{:S(2)}, u32[]{:S(2)}) collective-permute-start(bf16[16,16,1664]{2,1,0:T(8,128)(2,1)S(1)} %collective-permute-done.5.refs_6_), channel_id=1, source_target_pairs={{4,0},{0,4},{5,1},{1,5},{6,2},{2,6},{7,3},{3,7},{12,8},{8,12},{13,... | collective-permute-start | bytes 2555912 | tf_op jit(solution)/shard_map/ppermute | solution.py:33
  75.8 6.7 %collective-permute-start.8 = (bf16[16,16,1664]{2,1,0:T(8,128)(2,1)S(1)}, bf16[16,16,1664]{2,1,0:T(8,128)(2,1)S(1)}, u32[]{:S(2)}, u32[]{:S(2)}) collective-permute-start(bf16[16,16,1664]{2,1,0:T(8,128)(2,1)S(1)} %collective-permute-done.4.refs_5_), channel_id=1, source_target_pairs={{4,0},{0,4},{5,1},{1,5},{6,2},{2,6},{7,3},{3,7},{12,8},{8,12},{13,... | collective-permute-start | bytes 2555912 | tf_op jit(solution)/shard_map/ppermute | solution.py:33
  82.5 1.9 %collective-permute-start.7 = (bf16[16,16,1664]{2,1,0:T(8,128)(2,1)S(1)}, bf16[16,16,1664]{2,1,0:T(8,128)(2,1)S(1)}, u32[]{:S(2)}, u32[]{:S(2)}) collective-permute-start(bf16[16,16,1664]{2,1,0:T(8,128)(2,1)S(1)} %collective-permute-done.3.refs_4_), channel_id=1, source_target_pairs={{4,0},{0,4},{5,1},{1,5},{6,2},{2,6},{7,3},{3,7},{12,8},{8,12},{13,... | collective-permute-start | bytes 2555912 | tf_op jit(solution)/shard_map/ppermute | solution.py:33
  84.5 4.6 %collective-permute-start = (bf16[512,512]{1,0:T(8,128)(2,1)}, bf16[512,512]{1,0:T(8,128)(2,1)S(1)}, u32[]{:S(2)}, u32[]{:S(2)}) collective-permute-start(bf16[512,512]{1,0:T(8,128)(2,1)} %refs_0_.1), channel_id=1, source_target_pairs={{1,0},{2,1},{3,2},{0,3},{5,4},{6,5},{7,6},{4,7},{9,8},{10,9},{11,1... | collective-permute-start | bytes 1572872 | tf_op jit(solution)/shard_map/ppermute | solution.py:33
  89.1 11.1 %collective-permute-done.refs_1_ = bf16[512,512]{1,0:T(8,128)(2,1)S(1)} collective-permute-done((bf16[512,512]{1,0:T(8,128)(2,1)}, bf16[512,512]{1,0:T(8,128)(2,1)S(1)}, u32[]{:S(2)}, u32[]{:S(2)}) %collective-permute-start) | collective-permute-done | bytes 524320 | tf_op jit(solution)/shard_map/ppermute | solution.py:33
  100.2 1.0 copy-done
  101.9 1.4 shard_map.131.refs_0_
  103.4 4.0 %shard_map.132 = (bf16[512,384]{1,0:T(8,128)(2,1)S(1)}, bf16[512,256]{1,0:T(8,128)(2,1)S(1)}, f32[512,256]{1,0:T(8,128)S(1)}, bf16[2048,512]{1,0:T(8,128)(2,1)S(1)}) custom-call(bf16[512,2048]{1,0:T(8,128)(2,1)S(1)} %shard_map.131.refs_0_, f32[512,128]{1,0:T(8,128)S(1)} %get-tuple-element.37.refs_1_, f32[512,128]{1,0:T(8,128)S(1)} %get-tuple-element.36.refs_2_, ...), custom_call_target="tpu_custom_call" | custom-call | flops 2415919104 | bytes 8000000 | tf_op jit(solution)/shard_map/pallas_call | solution.py:130
  107.4 3.3 %collective-permute-start.11 = (bf16[128,384]{1,0:T(8,128)(2,1)S(1)}, bf16[128,384]{1,0:T(8,128)(2,1)S(1)}, u32[]{:S(2)}, u32[]{:S(2)}) collective-permute-start(bf16[128,384]{1,0:T(8,128)(2,1)S(1)} %get-tuple-element.32), channel_id=1, source_target_pairs={{4,0},{8,4},{12,8},{16,12},{20,16},{24,20},{28,24},{32,28},{36,32}... | collective-permute-start | bytes 294920 | tf_op jit(solution)/shard_map/ppermute | solution.py:317
  110.7 3.5 %collective-permute-start.10 = (bf16[128,384]{1,0:T(8,128)(2,1)S(1)}, bf16[128,384]{1,0:T(8,128)(2,1)S(1)}, u32[]{:S(2)}, u32[]{:S(2)}) collective-permute-start(bf16[128,384]{1,0:T(8,128)(2,1)S(1)} %get-tuple-element.33), channel_id=1, source_target_pairs={{0,4},{4,8},{8,12},{12,16},{16,20},{20,24},{24,28},{28,32},{32,36}... | collective-permute-start | bytes 294920 | tf_op jit(solution)/shard_map/ppermute | solution.py:316
  114.2 2.1 %shard_map.133 = (bf16[256,256]{1,0:T(8,128)(2,1)S(1)}, f32[256,4]{1,0:T(8,128)S(1)}) custom-call(f32[4]{0:T(128)S(1)} %copy-done.3, bf16[512,256]{1,0:T(8,128)(2,1)S(1)} %get-tuple-element.17.query_ref, bf16[512,384]{1,0:T(8,128)(2,1)S(1)} %get-tuple-element.18.kvc_ref), custom_call_target="tpu_custom_call" | custom-call | flops 2013265920 | bytes 2000000 | tf_op jit(solution)/shard_map/pallas_call | solution.py:205
  116.4 2.9 %shard_map.134 = (bf16[2,128,1024]{2,1,0:T(8,128)(2,1)S(1)}, bf16[512,512]{1,0:T(8,128)(2,1)S(1)}, f32[256,4]{1,0:T(8,128)S(1)}) custom-call(f32[4]{0:T(128)S(1)} %copy-done.3, bf16[512,256]{1,0:T(8,128)(2,1)S(1)} %get-tuple-element.17.query_ref, bf16[512,384]{1,0:T(8,128)(2,1)S(1)} %get-tuple-element.18.kvc_ref, ...), custom_call_target="tpu_custom_call" | custom-call | flops 1073741824 | bytes 8000000 | tf_op jit(solution)/shard_map/pallas_call | solution.py:296
  119.3 5.2 %collective-permute-start.13 = (bf16[128,1024]{1,0:T(8,128)(2,1)S(1)}, bf16[128,1024]{1,0:T(8,128)(2,1)S(1)}, u32[]{:S(2)}, u32[]{:S(2)}) collective-permute-start(bf16[128,1024]{1,0:T(8,128)(2,1)S(1)} %get-tuple-element.30), channel_id=1, source_target_pairs={{1,0},{2,1},{3,2},{0,3},{5,4},{6,5},{7,6},{4,7},{9,8},{10,9},{11,1... | collective-permute-start | bytes 786440 | tf_op jit(solution)/shard_map/ppermute | solution.py:33
  124.5 1.9 %collective-permute-start.12 = (bf16[128,1024]{1,0:T(8,128)(2,1)S(1)}, bf16[128,1024]{1,0:T(8,128)(2,1)S(1)}, u32[]{:S(2)}, u32[]{:S(2)}) collective-permute-start(bf16[128,1024]{1,0:T(8,128)(2,1)S(1)} %get-tuple-element.31), channel_id=1, source_target_pairs={{3,0},{0,1},{1,2},{2,3},{7,4},{4,5},{5,6},{6,7},{11,8},{8,9},{9,10... | collective-permute-start | bytes 786440 | tf_op jit(solution)/shard_map/ppermute | solution.py:33
  126.4 3.5 %collective-permute-done.13.high_ref = bf16[128,1024]{1,0:T(8,128)(2,1)S(1)} collective-permute-done((bf16[128,1024]{1,0:T(8,128)(2,1)S(1)}, bf16[128,1024]{1,0:T(8,128)(2,1)S(1)}, u32[]{:S(2)}, u32[]{:S(2)}) %collective-permute-start.13) | collective-permute-done | bytes 262176 | tf_op jit(solution)/shard_map/ppermute | solution.py:33
  130.0 5.3 %collective-permute-done.12.low_ref = bf16[128,1024]{1,0:T(8,128)(2,1)S(1)} collective-permute-done((bf16[128,1024]{1,0:T(8,128)(2,1)S(1)}, bf16[128,1024]{1,0:T(8,128)(2,1)S(1)}, u32[]{:S(2)}, u32[]{:S(2)}) %collective-permute-start.12) | collective-permute-done | bytes 262176 | tf_op jit(solution)/shard_map/ppermute | solution.py:33
  135.3 1.6 %shard_map.136 = (bf16[128,2048]{1,0:T(8,128)(2,1)}, bf16[128,2048]{1,0:T(8,128)(2,1)S(1)}) custom-call(bf16[512,512]{1,0:T(8,128)(2,1)S(1)} %get-tuple-element.22.both_ref, bf16[2048,512]{1,0:T(8,128)(2,1)S(1)} %get-tuple-element.21.out_rows_ref, bf16[128,1024]{1,0:T(8,128)(2,1)S(1)} %collective-permute-done.12.low_ref, ...), custom_call_target="tpu_custom_call" | custom-call | flops 536870912 | bytes 3000000 | tf_op jit(solution)/shard_map/pallas_call | solution.py:283
  136.9 1.9 %collective-permute-start.14 = (bf16[128,2048]{1,0:T(8,128)(2,1)}, bf16[128,2048]{1,0:T(8,128)(2,1)}, u32[]{:S(2)}, u32[]{:S(2)}) collective-permute-start(bf16[128,2048]{1,0:T(8,128)(2,1)} %get-tuple-element.24), channel_id=1, source_target_pairs={{3,0},{0,1},{1,2},{2,3},{7,4},{4,5},{5,6},{6,7},{11,8},{8,9},{9,10... | collective-permute-start | bytes 1572872 | tf_op jit(solution)/shard_map/ppermute | solution.py:33
  138.8 4.6 %collective-permute-start.15 = (bf16[128,2048]{1,0:T(8,128)(2,1)S(1)}, bf16[128,2048]{1,0:T(8,128)(2,1)}, u32[]{:S(2)}, u32[]{:S(2)}) collective-permute-start(bf16[128,2048]{1,0:T(8,128)(2,1)S(1)} %get-tuple-element.25), channel_id=1, source_target_pairs={{1,0},{2,1},{3,2},{0,3},{5,4},{6,5},{7,6},{4,7},{9,8},{10,9},{11,1... | collective-permute-start | bytes 1572872 | tf_op jit(solution)/shard_map/ppermute | solution.py:33
  143.7 0.8 shard_map.135
  145.1 8.4 %collective-permute-done.14 = bf16[128,2048]{1,0:T(8,128)(2,1)} collective-permute-done((bf16[128,2048]{1,0:T(8,128)(2,1)}, bf16[128,2048]{1,0:T(8,128)(2,1)}, u32[]{:S(2)}, u32[]{:S(2)}) %collective-permute-start.14) | collective-permute-done | bytes 524320 | tf_op jit(solution)/shard_map/ppermute | solution.py:33
  154.1 2.2 %add_convert_fusion = bf16[128,2048]{1,0:T(8,128)(2,1)} fusion(bf16[128,2048]{1,0:T(8,128)(2,1)} %collective-permute-done.15, bf16[128,2048]{1,0:T(8,128)(2,1)} %collective-permute-done.14, bf16[128,2048]{1,0:T(8,128)(2,1)S(1)} %shard_map.135), kind=kLoop, calls=%fused_computation | loop fusion | flops 1572864 | bytes 2097152 | tf_op jit(solution)/shard_map/convert_element_type | solution.py:382
  (33 shorter events, 2.3 us)
Async XLA Ops:
  36.9 37.0 %collective-permute-start.5 = (bf16[16,16,1664]{2,1,0:T(8,128)(2,1)S(1)}, bf16[16,16,1664]{2,1,0:T(8,128)(2,1)S(1)}, u32[]{:S(2)}, u32[]{:S(2)}) collective-permute-start(bf16[16,16,1664]{2,1,0:T(8,128)(2,1)S(1)} %bitcast.10), channel_id=1, source_target_pairs={{24,0},{0,8},{8,16},{16,24},{25,1},{1,9},{9,17},{17,25},{26,2},{2,... | collective-permute-start | bytes 2555912 | tf_op jit(solution)/shard_map/ppermute | solution.py:33
  40.0 35.8 %collective-permute-start.4 = (bf16[16,16,1664]{2,1,0:T(8,128)(2,1)S(1)}, bf16[16,16,1664]{2,1,0:T(8,128)(2,1)S(1)}, u32[]{:S(2)}, u32[]{:S(2)}) collective-permute-start(bf16[16,16,1664]{2,1,0:T(8,128)(2,1)S(1)} %bitcast.11), channel_id=1, source_target_pairs={{16,0},{24,8},{0,16},{8,24},{17,1},{25,9},{1,17},{9,25},{18,2},{26... | collective-permute-start | bytes 2555912 | tf_op jit(solution)/shard_map/ppermute | solution.py:33
  44.4 38.1 %collective-permute-start.3 = (bf16[16,16,1664]{2,1,0:T(8,128)(2,1)S(1)}, bf16[16,16,1664]{2,1,0:T(8,128)(2,1)S(1)}, u32[]{:S(2)}, u32[]{:S(2)}) collective-permute-start(bf16[16,16,1664]{2,1,0:T(8,128)(2,1)S(1)} %bitcast.12), channel_id=1, source_target_pairs={{8,0},{16,8},{24,16},{0,24},{9,1},{17,9},{25,17},{1,25},{10,2},{18... | collective-permute-start | bytes 2555912 | tf_op jit(solution)/shard_map/ppermute | solution.py:33
  47.5 11.7 %collective-permute-start.2 = (bf16[512,512]{1,0:T(8,128)(2,1)}, bf16[512,512]{1,0:T(8,128)(2,1)S(1)}, u32[]{:S(2)}, u32[]{:S(2)}) collective-permute-start(bf16[512,512]{1,0:T(8,128)(2,1)} %refs_0_.1), channel_id=1, source_target_pairs={{3,0},{0,1},{1,2},{2,3},{7,4},{4,5},{5,6},{6,7},{11,8},{8,9},{9,10... | collective-permute-start | bytes 1572872 | tf_op jit(solution)/shard_map/ppermute | solution.py:33
  50.7 33.8 %collective-permute-start.1 = (bf16[512,512]{1,0:T(8,128)(2,1)}, bf16[512,512]{1,0:T(8,128)(2,1)S(1)}, u32[]{:S(2)}, u32[]{:S(2)}) collective-permute-start(bf16[512,512]{1,0:T(8,128)(2,1)} %refs_0_.1), channel_id=1, source_target_pairs={{2,0},{3,1},{0,2},{1,3},{6,4},{7,5},{4,6},{5,7},{10,8},{11,9},{8,1... | collective-permute-start | bytes 1572872 | tf_op jit(solution)/shard_map/ppermute | solution.py:33
  59.2 44.2 %collective-permute-start.6 = (bf16[16,16,1664]{2,1,0:T(8,128)(2,1)S(1)}, bf16[16,16,1664]{2,1,0:T(8,128)(2,1)S(1)}, u32[]{:S(2)}, u32[]{:S(2)}) collective-permute-start(bf16[16,16,1664]{2,1,0:T(8,128)(2,1)S(1)} %bitcast.13), channel_id=1, source_target_pairs={{4,0},{0,4},{5,1},{1,5},{6,2},{2,6},{7,3},{3,7},{12,8},{8,12},{13,... | collective-permute-start | bytes 2555912 | tf_op jit(solution)/shard_map/ppermute | solution.py:33
  73.9 29.5 %collective-permute-start.9 = (bf16[16,16,1664]{2,1,0:T(8,128)(2,1)S(1)}, bf16[16,16,1664]{2,1,0:T(8,128)(2,1)S(1)}, u32[]{:S(2)}, u32[]{:S(2)}) collective-permute-start(bf16[16,16,1664]{2,1,0:T(8,128)(2,1)S(1)} %collective-permute-done.5.refs_6_), channel_id=1, source_target_pairs={{4,0},{0,4},{5,1},{1,5},{6,2},{2,6},{7,3},{3,7},{12,8},{8,12},{13,... | collective-permute-start | bytes 2555912 | tf_op jit(solution)/shard_map/ppermute | solution.py:33
  75.8 27.6 %collective-permute-start.8 = (bf16[16,16,1664]{2,1,0:T(8,128)(2,1)S(1)}, bf16[16,16,1664]{2,1,0:T(8,128)(2,1)S(1)}, u32[]{:S(2)}, u32[]{:S(2)}) collective-permute-start(bf16[16,16,1664]{2,1,0:T(8,128)(2,1)S(1)} %collective-permute-done.4.refs_5_), channel_id=1, source_target_pairs={{4,0},{0,4},{5,1},{1,5},{6,2},{2,6},{7,3},{3,7},{12,8},{8,12},{13,... | collective-permute-start | bytes 2555912 | tf_op jit(solution)/shard_map/ppermute | solution.py:33
  82.5 20.9 %collective-permute-start.7 = (bf16[16,16,1664]{2,1,0:T(8,128)(2,1)S(1)}, bf16[16,16,1664]{2,1,0:T(8,128)(2,1)S(1)}, u32[]{:S(2)}, u32[]{:S(2)}) collective-permute-start(bf16[16,16,1664]{2,1,0:T(8,128)(2,1)S(1)} %collective-permute-done.3.refs_4_), channel_id=1, source_target_pairs={{4,0},{0,4},{5,1},{1,5},{6,2},{2,6},{7,3},{3,7},{12,8},{8,12},{13,... | collective-permute-start | bytes 2555912 | tf_op jit(solution)/shard_map/ppermute | solution.py:33
  84.5 15.7 %collective-permute-start = (bf16[512,512]{1,0:T(8,128)(2,1)}, bf16[512,512]{1,0:T(8,128)(2,1)S(1)}, u32[]{:S(2)}, u32[]{:S(2)}) collective-permute-start(bf16[512,512]{1,0:T(8,128)(2,1)} %refs_0_.1), channel_id=1, source_target_pairs={{1,0},{2,1},{3,2},{0,3},{5,4},{6,5},{7,6},{4,7},{9,8},{10,9},{11,1... | collective-permute-start | bytes 1572872 | tf_op jit(solution)/shard_map/ppermute | solution.py:33
  100.2 1.0 copy-start
  101.2 0.7 copy-start.1
  103.4 10.9 %copy-start.3 = (f32[4]{0:T(128)S(1)}, f32[4]{0:T(128)}, u32[]{:S(2)}) copy-start(f32[4]{0:T(128)} %sink_ref.3) | copy-start | bytes 52
  107.4 8.9 %collective-permute-start.11 = (bf16[128,384]{1,0:T(8,128)(2,1)S(1)}, bf16[128,384]{1,0:T(8,128)(2,1)S(1)}, u32[]{:S(2)}, u32[]{:S(2)}) collective-permute-start(bf16[128,384]{1,0:T(8,128)(2,1)S(1)} %get-tuple-element.32), channel_id=1, source_target_pairs={{4,0},{8,4},{12,8},{16,12},{20,16},{24,20},{28,24},{32,28},{36,32}... | collective-permute-start | bytes 294920 | tf_op jit(solution)/shard_map/ppermute | solution.py:317
  110.7 5.6 %collective-permute-start.10 = (bf16[128,384]{1,0:T(8,128)(2,1)S(1)}, bf16[128,384]{1,0:T(8,128)(2,1)S(1)}, u32[]{:S(2)}, u32[]{:S(2)}) collective-permute-start(bf16[128,384]{1,0:T(8,128)(2,1)S(1)} %get-tuple-element.33), channel_id=1, source_target_pairs={{0,4},{4,8},{8,12},{12,16},{16,20},{20,24},{24,28},{28,32},{32,36}... | collective-permute-start | bytes 294920 | tf_op jit(solution)/shard_map/ppermute | solution.py:316
  114.2 2.1 %copy-start.2 = (f32[3,256]{1,0:T(4,128)S(1)}, f32[3,256]{1,0:T(4,128)}, u32[]{:S(2)}) copy-start(f32[3,256]{1,0:T(4,128)} %taps_ref.1) | copy-start | bytes 9220
  119.3 10.7 %collective-permute-start.13 = (bf16[128,1024]{1,0:T(8,128)(2,1)S(1)}, bf16[128,1024]{1,0:T(8,128)(2,1)S(1)}, u32[]{:S(2)}, u32[]{:S(2)}) collective-permute-start(bf16[128,1024]{1,0:T(8,128)(2,1)S(1)} %get-tuple-element.30), channel_id=1, source_target_pairs={{1,0},{2,1},{3,2},{0,3},{5,4},{6,5},{7,6},{4,7},{9,8},{10,9},{11,1... | collective-permute-start | bytes 786440 | tf_op jit(solution)/shard_map/ppermute | solution.py:33
  124.5 10.8 %collective-permute-start.12 = (bf16[128,1024]{1,0:T(8,128)(2,1)S(1)}, bf16[128,1024]{1,0:T(8,128)(2,1)S(1)}, u32[]{:S(2)}, u32[]{:S(2)}) collective-permute-start(bf16[128,1024]{1,0:T(8,128)(2,1)S(1)} %get-tuple-element.31), channel_id=1, source_target_pairs={{3,0},{0,1},{1,2},{2,3},{7,4},{4,5},{5,6},{6,7},{11,8},{8,9},{9,10... | collective-permute-start | bytes 786440 | tf_op jit(solution)/shard_map/ppermute | solution.py:33
  136.9 16.5 %collective-permute-start.14 = (bf16[128,2048]{1,0:T(8,128)(2,1)}, bf16[128,2048]{1,0:T(8,128)(2,1)}, u32[]{:S(2)}, u32[]{:S(2)}) collective-permute-start(bf16[128,2048]{1,0:T(8,128)(2,1)} %get-tuple-element.24), channel_id=1, source_target_pairs={{3,0},{0,1},{1,2},{2,3},{7,4},{4,5},{5,6},{6,7},{11,8},{8,9},{9,10... | collective-permute-start | bytes 1572872 | tf_op jit(solution)/shard_map/ppermute | solution.py:33
  138.8 15.2 %collective-permute-start.15 = (bf16[128,2048]{1,0:T(8,128)(2,1)S(1)}, bf16[128,2048]{1,0:T(8,128)(2,1)}, u32[]{:S(2)}, u32[]{:S(2)}) collective-permute-start(bf16[128,2048]{1,0:T(8,128)(2,1)S(1)} %get-tuple-element.25), channel_id=1, source_target_pairs={{1,0},{2,1},{3,2},{0,3},{5,4},{6,5},{7,6},{4,7},{9,8},{10,9},{11,1... | collective-permute-start | bytes 1572872 | tf_op jit(solution)/shard_map/ppermute | solution.py:33
